TPU v7x, 32 devices: a whole 2x2x4 slice. The times are simulated.
32 devices in a mesh: grp: 2 (over y), ep: 4 (over z), tp: 4 (over x, core).
Axes of the slice: x: 2, y: 2, z: 4, core: 2. Of those that a mesh axis runs over, the one named last changes fastest.
Arguments:
- query_vectors: bfloat16 [4096, 2048], P(('grp', 'ep'), 'tp'), parts along dimension 0, may hold values from -6 to 6
- attend_lookup_vectors: bfloat16 [4096, 2048], P(('grp', 'ep'), 'tp'), parts along dimension 0, may hold values from -6 to 6
- attend_content_vectors: bfloat16 [4096, 2048], P(('grp', 'ep'), 'tp'), parts along dimension 0, may hold values from -6 to 6
- forget_speed_dependent: bfloat16 [4096, 2048], P(('grp', 'ep'), 'tp'), parts along dimension 0, may hold values from -3 to 3
- amend_speed_dependent: bfloat16 [4096, 2048], P(('grp', 'ep'), 'tp'), parts along dimension 0, may hold values from -6 to 6
- result_switch_preactivation: bfloat16 [4096, 2048], P(('grp', 'ep'), 'tp'), parts along dimension 0, may hold values from -6 to 6
- feature_forget_baseline: float32 [2048], P('tp'), may hold values from -13 to -3
- amend_speed_baseline: float32 [2048], P('tp'), may hold values from -9 to 3
- sudden_forget_extra: float32 [4096, 32], P(('grp', 'ep'), 'tp'), parts along dimension 0, may hold values from -1 to 0
- group_scaling_factor: float32 [2048], P('tp'), may hold values from 0.1 to 1.9
- result_mapping_matrix: bfloat16 [2048, 2048], P('tp'), may hold values from -0.125 to 0.125
- specialist_tokens_activations: bfloat16 [4096, 2048], P(('grp', 'ep', 'tp')), parts along dimension 0, may hold values from -6 to 6
- specialist_scaling_factor: float32 [2048], replicated, may hold values from 0.1 to 1.9
- selected_specialists: int32 [4096, 2], P(('grp', 'ep', 'tp')), parts along dimension 0, may hold values from 0 to 3, all different within a row; in each aligned block of 128 rows (0 to 127, 128 to 255, ...) at most 96 rows name the same one
- selection_mixing_factors: float32 [4096, 2], P(('grp', 'ep', 'tp')), parts along dimension 0, may hold values from 0.3 to 1.5
- dispatched_switch_matrix: bfloat16 [4, 2048, 1024], P('ep', None, 'tp'), may hold values from -0.125 to 0.125
- dispatched_raising_matrix: bfloat16 [4, 2048, 1024], P('ep', None, 'tp'), may hold values from -0.125 to 0.125
- dispatched_lowering_matrix: bfloat16 [4, 1024, 2048], P('ep', 'tp'), may hold values from -0.1875 to 0.1875
- common_switch_matrix: bfloat16 [2048, 512], P(None, 'tp'), may hold values from -0.125 to 0.125
- common_raising_matrix: bfloat16 [2048, 512], P(None, 'tp'), may hold values from -0.125 to 0.125
- common_lowering_matrix: bfloat16 [512, 2048], P('tp'), may hold values from -0.25 to 0.25
Outputs:
- attend_result_matrix: bfloat16 [4096, 2048], P(('grp', 'ep', 'tp')), parts along dimension 0
- moe_out: bfloat16 [4096, 2048], P(('grp', 'ep', 'tp')), parts along dimension 0
There are 2 independent parts, one for each index of `grp`. A program takes and returns all parts, laid end to end along the dimension named above; an argument that names none is the same for every part. Nothing has to cross between parts.
Inputs may be any that keep to these rules, and one draw needn't show every extreme that they name: `selected_specialists`: each row names 2 different experts. Among the rows of one device no expert is named more than 96 times, and in every draw some device names some expert exactly 96 times.
All inputs are finite; a program needn't handle non-finite values.
Results may differ from a plain program's by a relative error of at most 0.023.
Values may be sent and summed in bfloat16 or wider, within the bound.
A program may use at most 128 MiB of HBM per device.

v0:
```python
import functools
import math

import jax
import jax.numpy as jnp
from jax import lax
from jax.experimental import pallas as pl
from jax.experimental.pallas import tpu as pltpu
from jax.sharding import PartitionSpec as P

highest = lax.Precision.HIGHEST


NN = (((1,), (0,)), ((), ()))
NT = (((1,), (1,)), ((), ()))


def split_two(array_in):
    high = array_in.astype(jnp.bfloat16)
    return high, (array_in - high.astype(jnp.float32)).astype(jnp.bfloat16)


def dot_parts(left, right, dims):
    def one(x, y):
        return lax.dot_general(x, y, dims, preferred_element_type=jnp.float32)

    return one(left[0], right[0]) + (one(left[0], right[1]) + one(left[1], right[0]))


def dot3(left, right, dims=NN):
    return dot_parts(split_two(left), split_two(right), dims)


def span_kernel(
    heads, size, q_ref, k_ref, v_ref, f_ref, a_ref, fb_ref, ab_ref, extra_ref, out_ref, memory_ref
):
    span = q_ref.shape[0]

    @pl.when(pl.program_id(0) == 0)
    def _():
        row = lax.broadcasted_iota(jnp.int32, (2 * size, size), 0)
        col = lax.broadcasted_iota(jnp.int32, (2 * size, size), 1)
        start = jnp.where(row == col + size, 1.0, 0.0)
        for h in range(heads):
            memory_ref[h] = start

    row = lax.broadcasted_iota(jnp.int32, (span, span), 0)
    col = lax.broadcasted_iota(jnp.int32, (span, span), 1)
    eye = jnp.where(row == col, 1.0, 0.0)
    below = jnp.where(row >= col, 1.0, 0.0)
    row2 = lax.broadcasted_iota(jnp.int32, (2 * span, 2 * span), 0)
    col2 = lax.broadcasted_iota(jnp.int32, (2 * span, 2 * span), 1)
    col2 = jnp.where(col2 >= span, col2 - span, col2)
    pair_mask = jnp.where(row2 >= span, row2 - span + 1, row2) > col2
    levels = []
    width = 1
    while width < span:
        levels.append(
            (row // (2 * width) == col // (2 * width))
            & (row // width % 2 == 1)
            & (col // width % 2 == 0)
        )
        width *= 2

    q_all = q_ref[...].astype(jnp.float32)
    k_all = k_ref[...].astype(jnp.float32)
    v_all = v_ref[...].astype(jnp.float32)
    rate_all = jax.nn.sigmoid(ab_ref[...] + a_ref[...].astype(jnp.float32))
    speed = -jnp.exp(fb_ref[...] + f_ref[...].astype(jnp.float32))
    extra = extra_ref[...]
    decay_all = speed + jnp.concatenate(
        [jnp.broadcast_to(extra[:, h : h + 1], (span, size)) for h in range(heads)], axis=1
    )
    cum_all = jnp.dot(below, decay_all, precision=highest, preferred_element_type=jnp.float32)
    prev_all = cum_all - decay_all
    middle = cum_all[span // 2 : span // 2 + 1]
    last = cum_all[span - 1 : span]
    exp_prev_mid = jnp.exp(prev_all - middle)
    exp_cum_mid = jnp.exp(cum_all - middle)
    exp_mid_cum = jnp.exp(middle - cum_all)
    exp_prev = jnp.exp(prev_all)
    exp_cum = jnp.exp(cum_all)
    exp_tail = jnp.exp(last - cum_all)
    exp_last = jnp.exp(last)
    write_all = k_all * rate_all
    squares = k_all * k_all

    every = range(heads)

    def cut(array_in, h):
        return array_in[:, h * size : (h + 1) * size]

    norms = [lax.rsqrt(jnp.sum(cut(squares, h), -1, keepdims=True) + 1e-06) for h in every]
    unit_all = k_all * jnp.concatenate(
        [jnp.broadcast_to(n, (span, size)) for n in norms], axis=1
    )
    erase_all = unit_all * rate_all
    left_all = jnp.concatenate([-unit_all * exp_prev_mid, q_all * exp_cum_mid], axis=0)
    right_all = jnp.concatenate([erase_all * exp_mid_cum, write_all * exp_mid_cum], axis=0)
    read_all = jnp.concatenate([-unit_all * exp_prev, q_all * exp_cum], axis=0)
    tail_all = jnp.concatenate([erase_all * exp_tail, write_all * exp_tail], axis=0)
    left_all, right_all = split_two(left_all), split_two(right_all)
    read_all, tail_all = split_two(read_all), split_two(tail_all)

    def cut2(parts, h):
        return tuple(cut(part, h) for part in parts)

    pairs = [
        jnp.where(pair_mask, dot_parts(cut2(left_all, h), cut2(right_all, h), NT), 0.0)
        for h in every
    ]
    strict = [p[:span, :span] for p in pairs]
    solved = [eye + jnp.where(levels[0], s, 0.0) for s in strict]
    for level in levels[1:]:
        halves = [split_two(x) for x in solved]
        middles = [
            dot_parts(split_two(jnp.where(level, s, 0.0)), x, NN) for s, x in zip(strict, halves)
        ]
        solved = [
            x + dot_parts(xs, split_two(m), NN) for x, xs, m in zip(solved, halves, middles)
        ]
    memories = [memory_ref[h] for h in every]
    reads = [dot_parts(cut2(read_all, h), split_two(memories[h]), NT) for h in every]
    blank = jnp.zeros((span, size), jnp.float32)
    values = [jnp.concatenate([cut(v_all, h), blank], axis=1) for h in every]
    rights = [
        reads[h][:span] + dot3(pairs[h][:span, span:], values[h]) for h in every
    ]
    updates = [dot3(solved[h], rights[h]) for h in every]
    stacked = [jnp.concatenate([updates[h], values[h]], axis=0) for h in every]
    for h in every:
        out_ref[:, 2 * size * h : 2 * size * (h + 1)] = reads[h][span:] + dot3(
            pairs[h][span:], stacked[h]
        )
    for h in every:
        memory_ref[h] = memories[h] * cut(exp_last, h) + dot_parts(
            split_two(stacked[h].T), cut2(tail_all, h), NN
        )


def finish_kernel(
    heads, size, place_ref, parts_ref, flat_ref, gate_ref, gain_ref, mixed_ref, state_ref
):
    @pl.when(pl.program_id(0) == 0)
    def _():
        state_ref[...] = jnp.zeros_like(state_ref)

        @pl.loop(0, place_ref[0])
        def _(k):
            for h in range(heads):
                part = parts_ref[k, h]
                own = split_two(state_ref[h])
                carry = part[size:]
                moved = lax.dot_general(
                    own[0], carry, NN, preferred_element_type=jnp.float32
                ) + lax.dot_general(own[1], carry, NN, preferred_element_type=jnp.float32)
                state_ref[h] = moved + part[:size].astype(jnp.float32)

    centered_all = []
    for h in range(heads):
        flat = flat_ref[:, 2 * size * h : 2 * size * (h + 1)]
        head_out = flat[:, :size] + dot3(flat[:, size:], state_ref[h], NT)
        centered = head_out - jnp.mean(head_out, -1, keepdims=True)
        head_var = jnp.mean(centered * centered, -1, keepdims=True)
        centered_all.append(centered * lax.rsqrt(head_var + 0.00064))
    scaled = jnp.concatenate(centered_all, axis=1) * gain_ref[...]
    gate = jax.nn.sigmoid(gate_ref[...].astype(jnp.float32))
    mixed_ref[...] = (scaled * gate).astype(jnp.bfloat16)


def mixer_half(
    query_vectors,
    attend_lookup_vectors,
    attend_content_vectors,
    forget_speed_dependent,
    amend_speed_dependent,
    result_switch_preactivation,
    feature_forget_baseline,
    amend_speed_baseline,
    sudden_forget_extra,
    group_scaling_factor,
):
    tokens, mix_width = query_vectors.shape
    heads = sudden_forget_extra.shape[1]
    size = mix_width // heads
    span = math.gcd(tokens, 64)
    rows = pl.BlockSpec((span, mix_width), lambda i: (i, 0))
    whole_row = pl.BlockSpec((1, mix_width), lambda i: (0, 0))
    wide = pl.BlockSpec((span, 2 * mix_width), lambda i: (i, 0))
    serial = pltpu.CompilerParams(dimension_semantics=("arbitrary",))
    flat_out, memory_end = pl.pallas_call(
        functools.partial(span_kernel, heads, size),
        grid=(tokens // span,),
        in_specs=[
            rows,
            rows,
            rows,
            rows,
            rows,
            whole_row,
            whole_row,
            pl.BlockSpec((span, heads), lambda i: (i, 0)),
        ],
        out_specs=[wide, pl.BlockSpec((heads, 2 * size, size), lambda i: (0, 0, 0))],
        out_shape=[
            jax.ShapeDtypeStruct((tokens, 2 * mix_width), jnp.float32),
            jax.ShapeDtypeStruct((heads, 2 * size, size), jnp.float32),
        ],
        compiler_params=serial,
        cost_estimate=pl.CostEstimate(
            flops=100_000_000_000 // 2, bytes_accessed=5_000_000, transcendentals=0
        ),
        name="spans",
    )(
        query_vectors,
        attend_lookup_vectors,
        attend_content_vectors,
        forget_speed_dependent,
        amend_speed_dependent,
        feature_forget_baseline.reshape(1, mix_width),
        amend_speed_baseline.reshape(1, mix_width),
        sudden_forget_extra,
    )
    parts = lax.all_gather(memory_end.astype(jnp.bfloat16), "ep")
    place = lax.axis_index("ep").reshape(1).astype(jnp.int32)
    return pl.pallas_call(
        functools.partial(finish_kernel, heads, size),
        grid=(tokens // span,),
        in_specs=[
            pl.BlockSpec(memory_space=pltpu.SMEM),
            pl.BlockSpec(parts.shape, lambda i: (0, 0, 0, 0)),
            wide,
            rows,
            whole_row,
        ],
        out_specs=rows,
        out_shape=jax.ShapeDtypeStruct((tokens, mix_width), jnp.bfloat16),
        scratch_shapes=[pltpu.VMEM((heads, size, size), jnp.float32)],
        compiler_params=serial,
        cost_estimate=pl.CostEstimate(
            flops=10_000_000_000, bytes_accessed=4_000_000, transcendentals=0
        ),
        name="finish",
    )(
        place,
        parts,
        flat_out,
        result_switch_preactivation,
        group_scaling_factor.reshape(1, mix_width),
    )


def swiglu_rows(rows, gate_w, up_w):
    gate_vals = jnp.dot(rows, gate_w, preferred_element_type=jnp.float32)
    up_vals = jnp.dot(rows, up_w, preferred_element_type=jnp.float32)
    return (jax.nn.silu(gate_vals) * up_vals).astype(jnp.bfloat16)


def on_device(
    query_vectors,
    attend_lookup_vectors,
    attend_content_vectors,
    forget_speed_dependent,
    amend_speed_dependent,
    result_switch_preactivation,
    feature_forget_baseline,
    amend_speed_baseline,
    sudden_forget_extra,
    group_scaling_factor,
    result_mapping_matrix,
    specialist_tokens_activations,
    specialist_scaling_factor,
    selected_specialists,
    selection_mixing_factors,
    dispatched_switch_matrix,
    dispatched_raising_matrix,
    dispatched_lowering_matrix,
    common_switch_matrix,
    common_raising_matrix,
    common_lowering_matrix,
):
    mixed_rows = mixer_half(
        query_vectors,
        attend_lookup_vectors,
        attend_content_vectors,
        forget_speed_dependent,
        amend_speed_dependent,
        result_switch_preactivation,
        feature_forget_baseline,
        amend_speed_baseline,
        sudden_forget_extra,
        group_scaling_factor,
    )
    floats = specialist_tokens_activations.astype(jnp.float32)
    normed = (
        floats
        * lax.rsqrt(jnp.mean(floats * floats, -1, keepdims=True) + 1e-06)
        * specialist_scaling_factor
    )
    normed = normed.astype(jnp.bfloat16)
    tok_rows, top_count = selected_specialists.shape
    model_width = specialist_tokens_activations.shape[1]
    experts = lax.axis_size("ep")
    capacity = 3 * tok_rows * top_count // (2 * experts)
    flat_ids = selected_specialists.reshape(-1)
    one_hot = (flat_ids[:, None] == jnp.arange(experts, dtype=jnp.int32)[None, :]).astype(jnp.int32)
    slot_rank = jnp.sum((jnp.cumsum(one_hot, axis=0) - 1) * one_hot, axis=1)
    position = flat_ids * capacity + slot_rank
    placing = position[:, None] == jnp.arange(experts * capacity, dtype=jnp.int32)[None, :]
    placing = jnp.sum(
        placing.astype(jnp.bfloat16).reshape(tok_rows, top_count, experts * capacity), axis=1
    )
    outgoing = jnp.einsum("te,td->ed", placing, normed, preferred_element_type=jnp.float32).astype(
        jnp.bfloat16
    )
    gate_w = dispatched_switch_matrix[0]
    up_w = dispatched_raising_matrix[0]
    down_w = dispatched_lowering_matrix[0]
    received = lax.all_to_all(
        outgoing.reshape(experts, capacity, model_width),
        "ep",
        split_axis=0,
        concat_axis=0,
        tiled=True,
    )
    local_rows = experts * capacity
    hidden = swiglu_rows(
        lax.all_gather(received.reshape(local_rows, model_width), "tp", axis=0, tiled=True),
        gate_w,
        up_w,
    )
    summed = lax.psum_scatter(
        jnp.dot(hidden, down_w, preferred_element_type=jnp.float32).astype(jnp.bfloat16),
        "tp",
        scatter_dimension=0,
        tiled=True,
    )
    expert_out = lax.all_to_all(
        summed.reshape(experts, capacity, model_width),
        "ep",
        split_axis=0,
        concat_axis=0,
        tiled=True,
    ).reshape(experts * capacity, model_width)
    picked = jnp.take(expert_out, position, axis=0).astype(jnp.float32)
    routed = jnp.sum(
        (picked * selection_mixing_factors.reshape(-1)[:, None]).reshape(
            tok_rows, top_count, model_width
        ),
        axis=1,
    )
    shared_hidden = swiglu_rows(
        lax.all_gather(normed, "tp", axis=0, tiled=True),
        common_switch_matrix,
        common_raising_matrix,
    )
    attend_result_matrix = lax.psum_scatter(
        jnp.dot(mixed_rows, result_mapping_matrix, preferred_element_type=jnp.float32).astype(
            jnp.bfloat16
        ),
        "tp",
        scatter_dimension=0,
        tiled=True,
    )
    shared_sum = lax.psum_scatter(
        jnp.dot(shared_hidden, common_lowering_matrix, preferred_element_type=jnp.float32).astype(
            jnp.bfloat16
        ),
        "tp",
        scatter_dimension=0,
        tiled=True,
    ).astype(jnp.float32)
    moe_out = (routed + shared_sum).astype(jnp.bfloat16)
    return (attend_result_matrix, moe_out)


def solution(mesh):
    placed = (
        P(("grp", "ep"), "tp"),
        P(("grp", "ep"), "tp"),
        P(("grp", "ep"), "tp"),
        P(("grp", "ep"), "tp"),
        P(("grp", "ep"), "tp"),
        P(("grp", "ep"), "tp"),
        P("tp"),
        P("tp"),
        P(("grp", "ep"), "tp"),
        P("tp"),
        P("tp", None),
        P(("grp", "ep", "tp"), None),
        P(),
        P(("grp", "ep", "tp"), None),
        P(("grp", "ep", "tp"), None),
        P("ep", None, "tp"),
        P("ep", None, "tp"),
        P("ep", "tp", None),
        P(None, "tp"),
        P(None, "tp"),
        P("tp", None),
    )
    return jax.shard_map(
        on_device,
        mesh=mesh,
        in_specs=placed,
        out_specs=(P(("grp", "ep", "tp"), None), P(("grp", "ep", "tp"), None)),
        check_vma=False,
    )
```

profile of v0, /device:TPU:0, one launch (start us, length us, event | category | flops | bytes accessed | tf_op | source)
XLA Modules:
  0.0 263.5 jit_solution(17232832031391645483)
XLA Ops:
  7.2 0.9 copy.58
  8.3 0.1 reshape.125
  8.4 1.2 reduce-window.6
  10.1 0.1 reduce_sum.44
  10.3 0.7 compare_and_fusion
  11.1 1.2 fusion.2
  12.4 1.2 fusion.4
  13.6 0.6 convolution_convert_fusion.3
  14.2 43.2 %all_to_all.10 = bf16[4,96,2048]{2,1,0:T(8,128)(2,1)} all-to-all(bf16[4,96,2048]{2,1,0:T(8,128)(2,1)S(1)} %bitcast.48), channel_id=1, replica_groups=mesh['grp'=2,'ep'=4,'tp'=4] {'ep'}, dimensions={0} | all-to-all | bytes 3145728 | tf_op jit(solution)/shard_map/all_to_all | solution.py:319
  57.5 0.7 all-gather.6.cloned.1.call-update
  58.3 44.8 %all-gather.4.cloned.1.call-done = bf16[1536,2048]{1,0:T(8,128)(2,1)} async-done(((bf16[384,2048]{1,0:T(8,128)(2,1)}), bf16[1536,2048]{1,0:T(8,128)(2,1)}) %all-gather.4.cloned.1.call-update) | async-done | bytes 6291472 | tf_op jit(solution)/shard_map/all_gather | solution.py:328
  103.1 6.0 %fusion.8 = f32[1536,256]{1,0:T(8,128)} fusion(bf16[1536,2048]{1,0:T(8,128)(2,1)} %all-gather.4.cloned.1.call-done, bf16[1,2048,256]{2,1,0:T(8,128)(2,1)} %param.36), kind=kOutput, calls=%fused_computation.18 | convolution fusion | flops 1610612736 | bytes 8912896 | tf_op jit(solution)/shard_map/dot_general | solution.py:254
  109.1 12.9 %convolution_convert_fusion = bf16[1536,2048]{1,0:T(8,128)(2,1)} fusion(bf16[1536,2048]{1,0:T(8,128)(2,1)} %all-gather.4.cloned.1.call-done, f32[1536,256]{1,0:T(8,128)} %fusion.8, bf16[1,256,2048]{2,1,0:T(8,128)(2,1)S(1)} %copy-done.7, bf16[1,2048,256]{2,1,0:T(8,128)(2,1)} %param.37), kind=kOutput, calls=%fused_computation.1 | convolution fusion | flops 3226730496 | bytes 16252928 | tf_op jit(solution)/shard_map/dot_general | solution.py:333
  122.2 0.6 copy-done.4
  122.8 0.8 copy.55.extra_ref
  123.6 4.2 %all-gather.6.cloned.1.call-done = bf16[512,2048]{1,0:T(8,128)(2,1)} async-done(((bf16[128,2048]{1,0:T(8,128)(2,1)}), bf16[512,2048]{1,0:T(8,128)(2,1)}) %all-gather.6.cloned.1.call-update) | async-done | bytes 2097168 | tf_op jit(solution)/shard_map/all_gather | solution.py:353
  127.8 2.3 fusion.25
  130.1 5.3 %convolution_convert_fusion.1 = bf16[512,2048]{1,0:T(8,128)(2,1)} fusion(bf16[128,2048]{1,0:T(8,128)(2,1)S(1)} %copy-done.3, bf16[512,2048]{1,0:T(8,128)(2,1)} %all-gather.6.cloned.1.call-done, bf16[2048,128]{1,0:T(8,128)(2,1)} %param.40, f32[512,128]{1,0:T(8,128)S(1)} %fusion.25), kind=kOutput, calls=%fused_computation.2 | convolution fusion | flops 538312704 | bytes 5505024 | tf_op jit(solution)/shard_map/dot_general | solution.py:366
  135.5 0.2 reduce-scatter.4.cloned.1.call-start
  135.7 34.1 %spans.1 = (f32[512,1024]{1,0:T(8,128)}, f32[8,128,64]{2,1,0:T(8,128)}) custom-call(bf16[512,512]{1,0:T(8,128)(2,1)} %q_ref.1, bf16[512,512]{1,0:T(8,128)(2,1)} %k_ref.1, bf16[512,512]{1,0:T(8,128)(2,1)} %v_ref.1, bf16[512,512]{1,0:T(8,128)(2,1)} %f_ref.1, bf16[512,512]{1,0:T(8,128)(2,1)} %a_ref.1, f32[1,512]{1,0:T(1,128)} %bitcast.54, f32[1,512]{1,0:T(1,128)} %bitcast.55, ...), custom_call_target="tpu_custom_call" | custom-call | flops 49999998976 | bytes 5000000 | tf_op jit(solution)/shard_map/spans/pallas_call | solution.py:191
  169.8 1.1 convert_element_type.48
  171.1 16.1 %all-gather = bf16[32,128,64]{1,2,0:T(8,128)(2,1)S(1)} all-gather(bf16[8,128,64]{1,2,0:T(8,128)(2,1)S(1)} %copy.56), channel_id=2, replica_groups=mesh['grp'=2,'ep'=4,'tp'=4] {'ep'}, dimensions={0}, use_global_device_ids=true | all-gather | bytes 655360 | tf_op jit(solution)/shard_map/all_gather | solution.py:224
  187.2 1.4 copy.57
  188.5 8.4 %finish.1 = bf16[512,512]{1,0:T(8,128)(2,1)} custom-call(s32[1]{0:T(128)} %bitcast.place_ref, bf16[4,8,128,64]{3,2,1,0:T(8,128)(2,1)} %bitcast.50, f32[512,1024]{1,0:T(8,128)} %get-tuple-element.5.flat_ref, bf16[512,512]{1,0:T(8,128)(2,1)} %gate_ref.1, f32[1,512]{1,0:T(1,128)} %bitcast.56), custom_call_target="tpu_custom_call" | custom-call | flops 10000000000 | bytes 4000000 | tf_op jit(solution)/shard_map/finish/pallas_call | solution.py:226
  196.9 3.7 %convolution_convert_fusion.2 = bf16[512,2048]{1,0:T(8,128)(2,1)} fusion(bf16[512,512]{1,0:T(8,128)(2,1)} %finish.1, bf16[512,2048]{1,0:T(8,128)(2,1)S(1)} %copy-done), kind=kOutput, calls=%fused_computation.3 | convolution fusion | flops 1074790400 | bytes 4718592 | tf_op jit(solution)/shard_map/dot_general | solution.py:358
  200.7 5.6 %all-to-all-start.1 = ((bf16[4,96,2048]{2,1,0:T(8,128)(2,1)}), bf16[4,96,2048]{2,1,0:T(8,128)(2,1)}, u32[]{:S(2)}, u32[]{:S(2)}) async-start(bf16[4,96,2048]{2,1,0:T(8,128)(2,1)} %bitcast.49), calls=%async_computation.3 | async-start | bytes 3145728 | tf_op jit(solution)/shard_map/all_to_all | solution.py:338
  206.9 34.5 %all-to-all-done.1 = bf16[4,96,2048]{2,1,0:T(8,128)(2,1)} async-done(((bf16[4,96,2048]{2,1,0:T(8,128)(2,1)}), bf16[4,96,2048]{2,1,0:T(8,128)(2,1)}, u32[]{:S(2)}, u32[]{:S(2)}) %all-to-all-start.1) | async-done | bytes 1572896 | tf_op jit(solution)/shard_map/all_to_all | solution.py:338
  241.4 4.2 %gather_fusion = bf16[256,2048]{1,0:T(8,128)(2,1)S(1)} fusion(bf16[384,2048]{1,0:T(8,128)(2,1)} %bitcast.13, s32[1024]{0:T(1024)S(1)} %pad_clamp_fusion), kind=kCustom, calls=%fused_computation | custom fusion | bytes 2098176 | tf_op jit(solution)/shard_map/jit(_take)/gather | solution.py:345
  245.6 1.5 gather.7
  247.1 5.4 %multiply_reduce_fusion = f32[128,2048]{1,0:T(8,128)S(1)} fusion(bf16[128,2,2048]{2,1,0:T(2,128)(2,1)} %gather.7, pred[128,2]{1,0:T(8,128)(4,1)S(1)} %copy.63, f32[128,2]{1,0:T(8,128)S(1)} %copy.65), kind=kLoop, calls=%fused_computation.7 | loop fusion | flops 1835008 | bytes 2098432 | tf_op jit(solution)/shard_map/reduce_sum | solution.py:346
  252.5 1.9 add_convert_fusion
  254.5 2.5 reduce-scatter.4.cloned.1.call-done
  (45 shorter events, 1.7 us)
Async XLA Ops:
  7.2 189.7 %copy-start = (bf16[512,2048]{1,0:T(8,128)(2,1)S(1)}, bf16[512,2048]{1,0:T(8,128)(2,1)}, u32[]{:S(2)}) copy-start(bf16[512,2048]{1,0:T(8,128)(2,1)} %param.31) | copy-start | bytes 6291460
  7.2 95.9 %all-gather.4.cloned.1.call-start = ((), (), s32[]{:S(2)}) async-start(), calls=%async_computation.6 | async-start | bytes 7864320 | tf_op jit(solution)/shard_map/all_gather | solution.py:328
  13.6 43.8 %copy-start.1 = (bf16[128,2048]{1,0:T(8,128)(2,1)}, bf16[128,2048]{1,0:T(8,128)(2,1)S(1)}, u32[]{:S(2)}) copy-start(bf16[128,2048]{1,0:T(8,128)(2,1)S(1)} %fusion.4) | copy-start | bytes 1572868
  57.4 70.4 %all-gather.6.cloned.1.call-start = ((), (), s32[]{:S(2)}) async-start(), calls=%async_computation.8 | async-start | bytes 2621440 | tf_op jit(solution)/shard_map/all_gather | solution.py:353
  58.2 50.9 %copy-start.7 = (bf16[1,256,2048]{2,1,0:T(8,128)(2,1)S(1)}, bf16[1,256,2048]{2,1,0:T(8,128)(2,1)}, u32[]{:S(2)}) copy-start(bf16[1,256,2048]{2,1,0:T(8,128)(2,1)} %param.38) | copy-start | bytes 3145732
  58.2 142.5 %reduce-scatter.6.cloned.1.call-start = ((), (), s32[]{:S(2)}) async-start(), calls=%async_computation.7 | async-start | bytes 7864320 | tf_op jit(solution)/shard_map/reduce_scatter | solution.py:332
  122.1 0.7 copy-start.4
  122.1 5.8 %copy-start.2 = (bf16[2048,128]{1,0:T(8,128)(2,1)S(1)}, bf16[2048,128]{1,0:T(8,128)(2,1)}, u32[]{:S(2)}) copy-start(bf16[2048,128]{1,0:T(8,128)(2,1)} %param.39) | copy-start | bytes 1572868
  122.1 8.0 %copy-start.3 = (bf16[128,2048]{1,0:T(8,128)(2,1)S(1)}, bf16[128,2048]{1,0:T(8,128)(2,1)}, u32[]{:S(2)}) copy-start(bf16[128,2048]{1,0:T(8,128)(2,1)} %param.41) | copy-start | bytes 1572868
  122.1 130.4 %reduce-scatter.8.cloned.1.call-start = ((), (), s32[]{:S(2)}) async-start(), calls=%async_computation.9 | async-start | bytes 2621440 | tf_op jit(solution)/shard_map/reduce_scatter | solution.py:365
  135.5 121.5 %reduce-scatter.4.cloned.1.call-start = ((), (), s32[]{:S(2)}) async-start(), calls=%async_computation.5 | async-start | bytes 2621440 | tf_op jit(solution)/shard_map/reduce_scatter | solution.py:357
  200.6 5.7 %copy-start.5 = (s32[128,2]{0,1:T(2,128)S(1)}, s32[128,2]{0,1:T(2,128)}, u32[]{:S(2)}) copy-start(s32[128,2]{0,1:T(2,128)} %param.34) | copy-start | bytes 3076
  200.6 6.1 %copy-start.6 = (f32[128,2]{0,1:T(2,128)S(1)}, f32[128,2]{0,1:T(2,128)}, u32[]{:S(2)}) copy-start(f32[128,2]{0,1:T(2,128)} %param.35) | copy-start | bytes 3076
  200.7 40.7 %all-to-all-start.1 = ((bf16[4,96,2048]{2,1,0:T(8,128)(2,1)}), bf16[4,96,2048]{2,1,0:T(8,128)(2,1)}, u32[]{:S(2)}, u32[]{:S(2)}) async-start(bf16[4,96,2048]{2,1,0:T(8,128)(2,1)} %bitcast.49), calls=%async_computation.3 | async-start | bytes 3145728 | tf_op jit(solution)/shard_map/all_to_all | solution.py:338
Sparse Core Ops, SparseCore 0:
  57.6 45.4 all-gather.3
  105.2 22.5 all-gather.5
  130.4 58.8 reduce-scatter.5
  191.6 31.1 reduce-scatter.7
  225.8 31.1 reduce-scatter.3
where the time goes:
time: 264 us
  waiting for transfers between devices  86.9 us (33%)
  blocking collectives  59.3 us (22%)
  Pallas kernels  42.5 us (16%)
  matrix products  30.9 us (12%)
  between operations  14 us (5%)
  other arithmetic  13.1 us (5%)
  local copies, waits for them, and re-layouts  10.9 us (4%)
  starting transfers between devices  6.01 us (2%)
    all_gather x1, waiting for transfers between devices, on_device(): lax.all_gather(received.reshape(local_rows, model_width), 'tp', axis=0, t...  44.8 us
    all_to_all x1, blocking collectives, on_device(): lax.all_to_all(outgoing.reshape(experts, capacity, model_width), 'ep', sp...  43.2 us
    all_to_all x1, waiting for transfers between devices, on_device(): lax.all_to_all(summed.reshape(experts, capacity, model_width), 'ep', spli...  34.5 us
    pallas_call x1, Pallas kernels, mixer_half(): pl.pallas_call(functools.partial(span_kernel, heads, size), grid=(tokens...  34.1 us
    all_gather x1, blocking collectives, mixer_half(): parts = lax.all_gather(memory_end.astype(jnp.bfloat16), 'ep')  16.1 us
    dot_general x1, matrix products, on_device(): jnp.dot(hidden, down_w, preferred_element_type=jnp.float32)  12.9 us
    pallas_call x1, Pallas kernels, mixer_half(): pl.pallas_call(functools.partial(finish_kernel, heads, size), grid=(token...  8.36 us
    dot_general x2, matrix products, swiglu_rows(): gate_vals = jnp.dot(rows, gate_w, preferred_element_type=jnp.float32)  8.31 us
  transfers between devices with their start and end apart: 6, of which 4 were waited for; matrix products, arithmetic and copies ran while one was open for 18% of the time, Pallas kernels for 16%

commit v1 on v0

--- a/solution.py
+++ b/solution.py
@@ -256,7 +256,7 @@
     return (jax.nn.silu(gate_vals) * up_vals).astype(jnp.bfloat16)
 
 
-def on_device(
+def collective_plan(
     query_vectors,
     attend_lookup_vectors,
     attend_content_vectors,
@@ -374,6 +374,664 @@
     return (attend_result_matrix, moe_out)
 
 
+MESH = pl.DeviceIdType.MESH
+
+
+def span_step(heads, size, span, i, q_ref, k_ref, v_ref, f_ref, a_ref, fb_ref, ab_ref, extra_ref,
+              flat_ref, memory_ref):
+    here = pl.ds(pl.multiple_of(i * span, span), span)
+    row = lax.broadcasted_iota(jnp.int32, (span, span), 0)
+    col = lax.broadcasted_iota(jnp.int32, (span, span), 1)
+    eye = jnp.where(row == col, 1.0, 0.0)
+    below = jnp.where(row >= col, 1.0, 0.0)
+    row2 = lax.broadcasted_iota(jnp.int32, (2 * span, 2 * span), 0)
+    col2 = lax.broadcasted_iota(jnp.int32, (2 * span, 2 * span), 1)
+    col2 = jnp.where(col2 >= span, col2 - span, col2)
+    pair_mask = jnp.where(row2 >= span, row2 - span + 1, row2) > col2
+    levels = []
+    width = 1
+    while width < span:
+        levels.append(
+            (row // (2 * width) == col // (2 * width))
+            & (row // width % 2 == 1)
+            & (col // width % 2 == 0)
+        )
+        width *= 2
+
+    q_all = q_ref[here, :].astype(jnp.float32)
+    k_all = k_ref[here, :].astype(jnp.float32)
+    v_all = v_ref[here, :].astype(jnp.float32)
+    rate_all = jax.nn.sigmoid(ab_ref[...] + a_ref[here, :].astype(jnp.float32))
+    speed = -jnp.exp(fb_ref[...] + f_ref[here, :].astype(jnp.float32))
+    extra = extra_ref[here, :]
+    decay_all = speed + jnp.concatenate(
+        [jnp.broadcast_to(extra[:, h : h + 1], (span, size)) for h in range(heads)], axis=1
+    )
+    cum_all = jnp.dot(below, decay_all, precision=highest, preferred_element_type=jnp.float32)
+    prev_all = cum_all - decay_all
+    middle = cum_all[span // 2 : span // 2 + 1]
+    last = cum_all[span - 1 : span]
+    exp_prev_mid = jnp.exp(prev_all - middle)
+    exp_cum_mid = jnp.exp(cum_all - middle)
+    exp_mid_cum = jnp.exp(middle - cum_all)
+    exp_prev = jnp.exp(prev_all)
+    exp_cum = jnp.exp(cum_all)
+    exp_tail = jnp.exp(last - cum_all)
+    exp_last = jnp.exp(last)
+    write_all = k_all * rate_all
+    squares = k_all * k_all
+
+    every = range(heads)
+
+    def cut(array_in, h):
+        return array_in[:, h * size : (h + 1) * size]
+
+    norms = [lax.rsqrt(jnp.sum(cut(squares, h), -1, keepdims=True) + 1e-06) for h in every]
+    unit_all = k_all * jnp.concatenate(
+        [jnp.broadcast_to(n, (span, size)) for n in norms], axis=1
+    )
+    erase_all = unit_all * rate_all
+    left_all = jnp.concatenate([-unit_all * exp_prev_mid, q_all * exp_cum_mid], axis=0)
+    right_all = jnp.concatenate([erase_all * exp_mid_cum, write_all * exp_mid_cum], axis=0)
+    read_all = jnp.concatenate([-unit_all * exp_prev, q_all * exp_cum], axis=0)
+    tail_all = jnp.concatenate([erase_all * exp_tail, write_all * exp_tail], axis=0)
+    left_all, right_all = split_two(left_all), split_two(right_all)
+    read_all, tail_all = split_two(read_all), split_two(tail_all)
+
+    def cut2(parts, h):
+        return tuple(cut(part, h) for part in parts)
+
+    pairs = [
+        jnp.where(pair_mask, dot_parts(cut2(left_all, h), cut2(right_all, h), NT), 0.0)
+        for h in every
+    ]
+    strict = [p[:span, :span] for p in pairs]
+    solved = [eye + jnp.where(levels[0], s, 0.0) for s in strict]
+    for level in levels[1:]:
+        halves = [split_two(x) for x in solved]
+        middles = [
+            dot_parts(split_two(jnp.where(level, s, 0.0)), x, NN) for s, x in zip(strict, halves)
+        ]
+        solved = [
+            x + dot_parts(xs, split_two(m), NN) for x, xs, m in zip(solved, halves, middles)
+        ]
+    memories = [memory_ref[h] for h in every]
+    reads = [dot_parts(cut2(read_all, h), split_two(memories[h]), NT) for h in every]
+    blank = jnp.zeros((span, size), jnp.float32)
+    values = [jnp.concatenate([cut(v_all, h), blank], axis=1) for h in every]
+    rights = [
+        reads[h][:span] + dot3(pairs[h][:span, span:], values[h]) for h in every
+    ]
+    updates = [dot3(solved[h], rights[h]) for h in every]
+    stacked = [jnp.concatenate([updates[h], values[h]], axis=0) for h in every]
+    for h in every:
+        flat_ref[here, 2 * size * h : 2 * size * (h + 1)] = reads[h][span:] + dot3(
+            pairs[h][span:], stacked[h]
+        )
+    for h in every:
+        memory_ref[h] = memories[h] * cut(exp_last, h) + dot_parts(
+            split_two(stacked[h].T), cut2(tail_all, h), NN
+        )
+
+
+def whole_kernel(
+    cfg,
+    q_ref, k_ref, v_ref, f_ref, a_ref, fb_ref, ab_ref, extra_ref, gain_ref,
+    tok_ref, scale_ref, sel_ref, fac_ref,
+    gate_hbm, map_hbm, gw_hbm, uw_hbm, dw_hbm, cg_hbm, cu_hbm, cd_hbm,
+    mix_out, moe_out,
+    xg, wg, flat, memory, parts, state, mixed, mp, mc, mx,
+    part, rc, rx, zb, tb, acc,
+    gate_v, map_v, gw_v, uw_v, dw_v, cg_v, cu_v, cd_v,
+    local_sem,
+    agz_s, agz_r, agx_s, agx_r, agd_s, agd_r, w_s, w_r, st_s, st_r,
+    md_s, md_r, mx_s, mx_r, rd_s, rd_r, rx_s, rx_r, rz_s, rz_r,
+):
+    E, T, R, heads, size, span, steps = cfg
+    X = 2
+    D = xg.shape[1]
+    g = lax.axis_index("grp")
+    e = lax.axis_index("ep")
+    t = lax.axis_index("tp")
+    x = t // 2
+    c = t % 2
+    f32 = jnp.float32
+    bf16 = jnp.bfloat16
+    last = E - 1
+
+    def at(ee, xx, cc):
+        return (g, ee, 2 * xx + cc)
+
+    def block(ref, b):
+        return ref.at[pl.ds(pl.multiple_of(b * R, R), R)]
+
+    def index(ee, xx, cc):
+        return ee * T + 2 * xx + cc
+
+    def remote(src, dst, ssem, rsem, target):
+        return pltpu.make_async_remote_copy(
+            src_ref=src, dst_ref=dst, send_sem=ssem, recv_sem=rsem,
+            device_id=target, device_id_type=MESH,
+        )
+
+    barrier = pltpu.get_barrier_semaphore()
+    for de in range(E):
+        for dt in range(T):
+            if de or dt:
+                pl.semaphore_signal(
+                    barrier, inc=1, device_id=(g, (e + de) % E, (t + dt) % T), device_id_type=MESH
+                )
+    locals_ = [
+        pltpu.make_async_copy(a, b, local_sem.at[n])
+        for n, (a, b) in enumerate(
+            [
+                (gate_hbm, gate_v), (map_hbm, map_v), (gw_hbm, gw_v), (uw_hbm, uw_v),
+                (dw_hbm, dw_v), (cg_hbm, cg_v), (cu_hbm, cu_v), (cd_hbm, cd_v),
+            ]
+        )
+    ]
+    for copy in locals_:
+        copy.start()
+
+    mine = index(e, x, c)
+
+    @pl.loop(0, R // 16)
+    def _(r):
+        floats = tok_ref[pl.ds(pl.multiple_of(r * 16, 16), 16), :].astype(f32)
+        normed = (
+            floats
+            * lax.rsqrt(jnp.mean(floats * floats, -1, keepdims=True) + 1e-06)
+            * scale_ref[...]
+        )
+        xg[pl.ds(pl.multiple_of(mine * R + r * 16, 16), 16), :] = normed.astype(bf16)
+
+    lane = lax.broadcasted_iota(jnp.int32, (R, 128), 1)
+    weights = jnp.zeros((R, 128), f32)
+    for j in range(sel_ref.shape[1]):
+        weights = weights + jnp.where(lane == sel_ref[:, j : j + 1], fac_ref[:, j : j + 1], 0.0)
+    wrows = wg.shape[1]
+    wg[mine] = weights.T[:wrows]
+    pl.semaphore_wait(barrier, E * T - 1)
+
+    def zr(k):
+        b = index(e - k, x, c)
+        return remote(block(xg, b), block(xg, b), agz_s.at[0, k], agz_r.at[0, k], at(e + 1, x, c))
+
+    def zl(k):
+        b = index(e + k, x, c)
+        return remote(block(xg, b), block(xg, b), agz_s.at[1, k], agz_r.at[1, k], at(e - 1, x, c))
+
+    def xs(ee):
+        b = index(ee, x, c)
+        return remote(block(xg, b), block(xg, b), agx_s.at[ee], agx_r.at[ee], at(e, 1 - x, c))
+
+    def ds(ee, xx):
+        b = index(ee, xx, c)
+        n = ee * X + xx
+        return remote(block(xg, b), block(xg, b), agd_s.at[n], agd_r.at[n], at(e, x, 1 - c))
+
+    def zr_wait(k):
+        b = index(e - 1 - k, x, c)
+        remote(block(xg, b), block(xg, b), agz_s.at[0, k], agz_r.at[0, k], at(e, x, c)).wait_recv()
+
+    def zl_wait(k):
+        b = index(e + 1 + k, x, c)
+        remote(block(xg, b), block(xg, b), agz_s.at[1, k], agz_r.at[1, k], at(e, x, c)).wait_recv()
+
+    def xs_wait(ee):
+        b = index(ee, 1 - x, c)
+        remote(block(xg, b), block(xg, b), agx_s.at[ee], agx_r.at[ee], at(e, x, c)).wait_recv()
+
+    def ds_wait(ee, xx):
+        b = index(ee, xx, 1 - c)
+        n = ee * X + xx
+        remote(block(xg, b), block(xg, b), agd_s.at[n], agd_r.at[n], at(e, x, c)).wait_recv()
+
+    def gather_start():
+        pl.when(e < last)(lambda: zr(0).start())
+        pl.when(e > 0)(lambda: zl(0).start())
+        xs(e).start()
+        ds(e, x).start()
+
+    def gather_z(k):
+        @pl.when(e >= k + 1)
+        def _():
+            zr_wait(k)
+            if k + 1 < last:
+                pl.when(e < last)(lambda: zr(k + 1).start())
+            xs(e - 1 - k).start()
+            ds(e - 1 - k, x).start()
+
+        @pl.when(e + 1 + k <= last)
+        def _():
+            zl_wait(k)
+            if k + 1 < last:
+                pl.when(e > 0)(lambda: zl(k + 1).start())
+            xs(e + 1 + k).start()
+            ds(e + 1 + k, x).start()
+
+    def gather_x(k):
+        if k == 0:
+            xs_wait(e)
+            ds(e, 1 - x).start()
+        else:
+            @pl.when(e >= k)
+            def _():
+                xs_wait(e - k)
+                ds(e - k, 1 - x).start()
+
+            @pl.when(e + k <= last)
+            def _():
+                xs_wait(e + k)
+                ds(e + k, 1 - x).start()
+
+    def gather_sends_done():
+        for k in range(last):
+            pl.when((e < last) & (e >= k))(lambda: zr(k).wait_send())
+            pl.when((e > 0) & (e + k <= last))(lambda: zl(k).wait_send())
+        for ee in range(E):
+            xs(ee).wait_send()
+            for xx in range(X):
+                ds(ee, xx).wait_send()
+
+    def w_copy(de, dt):
+        n = de * T + dt - 1
+        return remote(
+            wg.at[mine], wg.at[mine], w_s.at[n], w_r.at[n], (g, (e + de) % E, (t + dt) % T)
+        )
+
+    def w_wait(de, dt):
+        n = de * T + dt - 1
+        b = ((e - de + E) % E) * T + (t - dt + T) % T
+        remote(wg.at[b], wg.at[b], w_s.at[n], w_r.at[n], at(e, x, c)).wait_recv()
+
+    others = [(de, dt) for de in range(E) for dt in range(T) if de or dt]
+    gather_start()
+    for de, dt in others:
+        w_copy(de, dt).start()
+
+    mrow = lax.broadcasted_iota(jnp.int32, (2 * size, size), 0)
+    mcol = lax.broadcasted_iota(jnp.int32, (2 * size, size), 1)
+    begin = jnp.where(mrow == mcol + size, 1.0, 0.0)
+    for h in range(heads):
+        memory[h] = begin
+
+    hop_at = [max(1, (3 * steps) // 8), max(1, (6 * steps) // 8)]
+
+    @pl.loop(0, steps)
+    def _(i):
+        for n, when in enumerate(hop_at):
+            if n < last:
+                @pl.when(i == when)
+                def _():
+                    gather_z(n)
+                    gather_x(n)
+        span_step(
+            heads, size, span, i, q_ref, k_ref, v_ref, f_ref, a_ref, fb_ref, ab_ref, extra_ref,
+            flat, memory,
+        )
+
+    for h in range(heads):
+        parts[e, h] = jnp.concatenate([memory[h, :size], memory[h, size:]], axis=1).astype(bf16)
+
+    def st_copy(d):
+        return remote(parts.at[e], parts.at[e], st_s.at[d - 1], st_r.at[d - 1], at(e + d, x, c))
+
+    def st_wait(d):
+        k = e - d
+        remote(parts.at[k], parts.at[k], st_s.at[d - 1], st_r.at[d - 1], at(e, x, c)).wait_recv()
+
+    for d in range(1, E):
+        pl.when(e + d <= last)(lambda: st_copy(d).start())
+    for k in range(len(hop_at), last):
+        gather_z(k)
+    state[...] = jnp.zeros_like(state)
+    for d in range(1, E):
+        pl.when(e >= d)(lambda: st_wait(d))
+
+    @pl.loop(0, e)
+    def _(k):
+        for h in range(heads):
+            piece = parts[k, h]
+            own = split_two(state[h])
+            carry = piece[:, size:]
+            moved = jnp.dot(own[0], carry, preferred_element_type=f32) + jnp.dot(
+                own[1], carry, preferred_element_type=f32
+            )
+            state[h] = moved + piece[:, :size].astype(f32)
+
+    locals_[0].wait()
+
+    @pl.loop(0, steps)
+    def _(i):
+        here = pl.ds(pl.multiple_of(i * span, span), span)
+        centered_all = []
+        for h in range(heads):
+            pane = flat[here, 2 * size * h : 2 * size * (h + 1)]
+            head_out = pane[:, :size] + dot3(pane[:, size:], state[h], NT)
+            centered = head_out - jnp.mean(head_out, -1, keepdims=True)
+            head_var = jnp.mean(centered * centered, -1, keepdims=True)
+            centered_all.append(centered * lax.rsqrt(head_var + 0.00064))
+        scaled = jnp.concatenate(centered_all, axis=1) * gain_ref[...]
+        gate = jax.nn.sigmoid(gate_v[here, :].astype(f32))
+        mixed[here, :] = (scaled * gate).astype(bf16)
+
+    for k in range(len(hop_at), E):
+        gather_x(k)
+
+    locals_[1].wait()
+
+    def md_copy(xx):
+        n = 2 * xx + 1 - c
+        return remote(block(mp, n), block(mc, xx), md_s.at[xx], md_r.at[xx], at(e, x, 1 - c))
+
+    def mx_copy():
+        n = 2 * (1 - x) + c
+        return remote(block(mp, n), mx, mx_s.at[0], mx_r.at[0], at(e, 1 - x, c))
+
+    def mixer_rows(n):
+        rows = mixed[pl.ds(pl.multiple_of(n * R, R), R), :]
+        for j in range(D // 512):
+            cols = slice(512 * j, 512 * (j + 1))
+            mp[pl.ds(pl.multiple_of(n * R, R), R), cols] = jnp.dot(
+                rows, map_v[:, cols], preferred_element_type=f32
+            ).astype(bf16)
+
+    @pl.loop(0, T)
+    def _(n):
+        order = jnp.where(n < X, 2 * n + 1 - c, 2 * (n - X) + c)
+        mixer_rows(order)
+
+    def add_rows(dst, terms, limit=16):
+        @pl.loop(0, R // limit)
+        def _(r):
+            here = pl.ds(pl.multiple_of(r * limit, limit), limit)
+            total = terms[0][here, :].astype(f32)
+            for term in terms[1:]:
+                total = total + term[here, :].astype(f32)
+            dst[here, :] = total.astype(dst.dtype)
+
+    for xx in range(X):
+        md_copy(xx).start()
+    for xx in range(X):
+        md_copy(xx).wait_recv()
+    away = block(mp, 2 * (1 - x) + c)
+    add_rows(away, [away, block(mc, 1 - x)])
+    mx_copy().start()
+
+    for copy in locals_[2:]:
+        copy.wait()
+    for ee in range(E):
+        for xx in range(X):
+            ds_wait(ee, xx)
+    for de, dt in others:
+        w_wait(de, dt)
+
+    def rd_copy(dest, xx):
+        n = dest * X + xx
+        return remote(
+            block(part, index(dest, xx, 1 - c)), block(rc, n), rd_s.at[n], rd_r.at[n],
+            at(e, x, 1 - c),
+        )
+
+    def rx_copy(dest):
+        return remote(
+            block(part, index(dest, 1 - x, c)), block(rx, dest), rx_s.at[dest], rx_r.at[dest],
+            at(e, 1 - x, c),
+        )
+
+    def expert_rows(dest, own):
+        wlane = lax.broadcasted_iota(jnp.int32, (R, wrows), 1)
+
+        @pl.loop(0, T // 2)
+        def _(half):
+            base = pl.multiple_of(dest * (T * R) + half * (2 * R), 2 * R)
+            rows = xg[pl.ds(base, 2 * R), :]
+            picked = []
+            for j in range(2):
+                table = wg[dest * T + half * 2 + j].T
+                picked.append(jnp.sum(jnp.where(wlane == e, table, 0.0), axis=1, keepdims=True))
+            column = jnp.concatenate(picked, axis=0)
+            gate_vals = jnp.dot(rows, gw_v[...], preferred_element_type=f32)
+            up_vals = jnp.dot(rows, uw_v[...], preferred_element_type=f32)
+            hidden = (jax.nn.silu(gate_vals) * up_vals * column).astype(bf16)
+            if own:
+                sg = jnp.dot(rows, cg_v[...], preferred_element_type=f32)
+                su = jnp.dot(rows, cu_v[...], preferred_element_type=f32)
+                shared = (jax.nn.silu(sg) * su).astype(bf16)
+            for j in range(D // 256):
+                cols = slice(256 * j, 256 * (j + 1))
+                total = jnp.dot(hidden, dw_v[:, cols], preferred_element_type=f32)
+                if own:
+                    total = total + jnp.dot(shared, cd_v[:, cols], preferred_element_type=f32)
+                part[pl.ds(base, 2 * R), cols] = total.astype(bf16)
+
+    def dest_of(k):
+        low = jnp.where(k < last - e, last - k, k - (last - e))
+        high = jnp.where(k < e, k, last - (k - e))
+        return jnp.where(k == last, e, jnp.where(e < E // 2, low, high))
+
+    def fold_core(dest):
+        rd_copy(dest, 1 - x).wait_recv()
+        there = block(part, index(dest, 1 - x, c))
+        add_rows(there, [there, block(rc, dest * X + 1 - x)])
+        rx_copy(dest).start()
+
+    @pl.loop(0, last)
+    def _(k):
+        dest = dest_of(k)
+        expert_rows(dest, False)
+        for xx in range(X):
+            rd_copy(dest, xx).start()
+
+        @pl.when(k > 0)
+        def _():
+            fold_core(dest_of(k - 1))
+
+    expert_rows(e, True)
+    for xx in range(X):
+        rd_copy(e, xx).start()
+    fold_core(dest_of(last - 1))
+    fold_core(e)
+
+    def z_step(k):
+        dest = dest_of(k)
+        up = jnp.where(dest > e, 1, 0)
+        n = up * E + dest
+        has_prev = jnp.where(dest > e, e > 0, e < last)
+        copy = remote(
+            block(tb, dest), block(zb, n), rz_s.at[n], rz_r.at[n], at(e + 2 * up - 1, x, c)
+        )
+        rd_copy(dest, x).wait_recv()
+        rx_copy(dest).wait_recv()
+        terms = [block(part, index(dest, x, c)), block(rc, dest * X + x), block(rx, dest)]
+
+        @pl.when(has_prev)
+        def _():
+            copy.wait_recv()
+            add_rows(block(tb, dest), terms + [block(zb, n)])
+
+        @pl.when(jnp.logical_not(has_prev))
+        def _():
+            add_rows(block(tb, dest), terms)
+
+        copy.start()
+
+    pl.loop(0, last)(z_step)
+
+    mx_copy().wait_recv()
+    add_rows(mix_out, [block(mp, 2 * x + c), block(mc, x), mx])
+    rd_copy(e, x).wait_recv()
+    rx_copy(e).wait_recv()
+    add_rows(acc, [block(part, index(e, x, c)), block(rc, e * X + x), block(rx, e)])
+    for up in range(2):
+        n = up * E + e
+        copy = remote(block(tb, e), block(zb, n), rz_s.at[n], rz_r.at[n], at(e, x, c))
+
+        @pl.when(e > 0 if up else e < last)
+        def _():
+            copy.wait_recv()
+            add_rows(acc, [acc, block(zb, n)])
+
+    add_rows(moe_out, [acc])
+
+    gather_sends_done()
+    for de, dt in others:
+        w_copy(de, dt).wait_send()
+    for d in range(1, E):
+        pl.when(e + d <= last)(lambda: st_copy(d).wait_send())
+    for xx in range(X):
+        md_copy(xx).wait_send()
+    mx_copy().wait_send()
+
+    @pl.loop(0, E)
+    def _(dest):
+        for xx in range(X):
+            rd_copy(dest, xx).wait_send()
+        rx_copy(dest).wait_send()
+
+    @pl.loop(0, last)
+    def _(k):
+        dest = dest_of(k)
+        up = jnp.where(dest > e, 1, 0)
+        n = up * E + dest
+        remote(
+            block(tb, dest), block(zb, n), rz_s.at[n], rz_r.at[n], at(e + 2 * up - 1, x, c)
+        ).wait_send()
+
+
+def on_device(
+    query_vectors,
+    attend_lookup_vectors,
+    attend_content_vectors,
+    forget_speed_dependent,
+    amend_speed_dependent,
+    result_switch_preactivation,
+    feature_forget_baseline,
+    amend_speed_baseline,
+    sudden_forget_extra,
+    group_scaling_factor,
+    result_mapping_matrix,
+    specialist_tokens_activations,
+    specialist_scaling_factor,
+    selected_specialists,
+    selection_mixing_factors,
+    dispatched_switch_matrix,
+    dispatched_raising_matrix,
+    dispatched_lowering_matrix,
+    common_switch_matrix,
+    common_raising_matrix,
+    common_lowering_matrix,
+):
+    E = lax.axis_size("ep")
+    T = lax.axis_size("tp")
+    R, D = specialist_tokens_activations.shape
+    tokens, mix_width = query_vectors.shape
+    heads = sudden_forget_extra.shape[1]
+    size = mix_width // heads
+    span = math.gcd(tokens, 64)
+    ff = dispatched_switch_matrix.shape[2]
+    sff = common_switch_matrix.shape[1]
+    gathered = E * T * R * D * 2
+    if T != 4 or gathered > 12_000_000 or tokens != T * R or E < 2:
+        return collective_plan(
+            query_vectors,
+            attend_lookup_vectors,
+            attend_content_vectors,
+            forget_speed_dependent,
+            amend_speed_dependent,
+            result_switch_preactivation,
+            feature_forget_baseline,
+            amend_speed_baseline,
+            sudden_forget_extra,
+            group_scaling_factor,
+            result_mapping_matrix,
+            specialist_tokens_activations,
+            specialist_scaling_factor,
+            selected_specialists,
+            selection_mixing_factors,
+            dispatched_switch_matrix,
+            dispatched_raising_matrix,
+            dispatched_lowering_matrix,
+            common_switch_matrix,
+            common_raising_matrix,
+            common_lowering_matrix,
+        )
+    cfg = (E, T, R, heads, size, span, tokens // span)
+    bf16, f32 = jnp.bfloat16, jnp.float32
+    wrows = -(-E // 8) * 8
+    dma = pltpu.SemaphoreType.DMA
+    vmem = pl.BlockSpec(memory_space=pltpu.VMEM)
+    hbm = pl.BlockSpec(memory_space=pl.ANY)
+    scratch = [
+        pltpu.VMEM((E * T * R, D), bf16),
+        pltpu.VMEM((E * T, wrows, R), f32),
+        pltpu.VMEM((tokens, 2 * mix_width), f32),
+        pltpu.VMEM((heads, 2 * size, size), f32),
+        pltpu.VMEM((E, heads, size, 2 * size), bf16),
+        pltpu.VMEM((heads, size, size), f32),
+        pltpu.VMEM((tokens, mix_width), bf16),
+        pltpu.VMEM((T * R, D), bf16),
+        pltpu.VMEM((2 * R, D), bf16),
+        pltpu.VMEM((R, D), bf16),
+        pltpu.VMEM((E * T * R, D), bf16),
+        pltpu.VMEM((E * 2 * R, D), bf16),
+        pltpu.VMEM((E * R, D), bf16),
+        pltpu.VMEM((2 * E * R, D), bf16),
+        pltpu.VMEM((E * R, D), bf16),
+        pltpu.VMEM((R, D), f32),
+        pltpu.VMEM((tokens, mix_width), bf16),
+        pltpu.VMEM((mix_width, D), bf16),
+        pltpu.VMEM((D, ff), bf16),
+        pltpu.VMEM((D, ff), bf16),
+        pltpu.VMEM((ff, D), bf16),
+        pltpu.VMEM((D, sff), bf16),
+        pltpu.VMEM((D, sff), bf16),
+        pltpu.VMEM((sff, D), bf16),
+        dma((8,)),
+        dma((2, E)), dma((2, E)), dma((E,)), dma((E,)), dma((2 * E,)), dma((2 * E,)),
+        dma((E * T,)), dma((E * T,)), dma((E,)), dma((E,)),
+        dma((2,)), dma((2,)), dma((1,)), dma((1,)),
+        dma((2 * E,)), dma((2 * E,)), dma((E,)), dma((E,)), dma((2 * E,)), dma((2 * E,)),
+    ]
+    return pl.pallas_call(
+        functools.partial(whole_kernel, cfg),
+        out_shape=(
+            jax.ShapeDtypeStruct((R, D), bf16),
+            jax.ShapeDtypeStruct((R, D), bf16),
+        ),
+        in_specs=[vmem] * 13 + [hbm] * 8,
+        out_specs=(vmem, vmem),
+        scratch_shapes=scratch,
+        compiler_params=pltpu.CompilerParams(
+            collective_id=0, has_side_effects=True, vmem_limit_bytes=66_000_000
+        ),
+        name="whole",
+    )(
+        query_vectors,
+        attend_lookup_vectors,
+        attend_content_vectors,
+        forget_speed_dependent,
+        amend_speed_dependent,
+        feature_forget_baseline.reshape(1, mix_width),
+        amend_speed_baseline.reshape(1, mix_width),
+        sudden_forget_extra,
+        group_scaling_factor.reshape(1, mix_width),
+        specialist_tokens_activations,
+        specialist_scaling_factor.reshape(1, D),
+        selected_specialists,
+        selection_mixing_factors,
+        result_switch_preactivation,
+        result_mapping_matrix,
+        dispatched_switch_matrix.reshape(D, ff),
+        dispatched_raising_matrix.reshape(D, ff),
+        dispatched_lowering_matrix.reshape(ff, D),
+        common_switch_matrix,
+        common_raising_matrix,
+        common_lowering_matrix,
+    )
+
+
 def solution(mesh):
     placed = (
         P(("grp", "ep"), "tp"),

time: 264 us -> 139 us (0.53)
  waiting for transfers between devices: 86.9 us -> 0 us
  Pallas kernels: 42.5 us -> 128 us
  blocking collectives: 59.3 us -> 0 us
  matrix products: 30.9 us -> 0 us
  between operations: 14 us -> 0.64 us
  other arithmetic: 13.1 us -> 0 us
  starting transfers between devices: 6.01 us -> 0 us
  local copies, waits for them, and re-layouts: 10.9 us -> 8.14 us
    pallas_call x2 -> x1, Pallas kernels: 42.5 us -> 128 us  [on_device(): pl.pallas_call(functools.partial(whole_kernel, cfg), out_shape=(jax.Shape...]
    all_gather x2 -> x0, waiting for transfers between devices: 49.1 us -> none  [the longest x1 44.8 us: on_device(): lax.all_gather(received.reshape(local_rows, model_width), 'tp', axis=0, t...]
    all_to_all x1 -> x0, blocking collectives: 43.2 us -> none  [on_device(): lax.all_to_all(outgoing.reshape(experts, capacity, model_width), 'ep', sp...]
    all_to_all x1 -> x0, waiting for transfers between devices: 34.5 us -> none  [on_device(): lax.all_to_all(summed.reshape(experts, capacity, model_width), 'ep', spli...]
    dot_general x6 -> x0, matrix products: 30.9 us -> none  [the longest x1 12.9 us: on_device(): jnp.dot(hidden, down_w, preferred_element_type=jnp.float32)]
    all_gather x1 -> x0, blocking collectives: 16.1 us -> none  [mixer_half(): parts = lax.all_gather(memory_end.astype(jnp.bfloat16), 'ep')]
    reduce_sum x4 -> x0, other arithmetic: 6.75 us -> none  [the longest x1 5.4 us: on_device(): jnp.sum((picked * selection_mixing_factors.reshape(-1)[:, None]).reshape(...]
    gather x2 -> x0, local copies, waits for them, and re-layouts: 5.68 us -> none  [on_device(): picked = jnp.take(expert_out, position, axis=0).astype(jnp.float32)]
  transfers between devices with their start and end apart: 6 -> 0, of which waited for: 4 -> 0; matrix products, arithmetic and copies ran while one was open for 18% -> 0% of each run, Pallas kernels for 16% -> 0%
where the time goes in v1:
time: 139 us; the launch traced here: 137 us
  Pallas kernels  128 us (92%)
  local copies, waits for them, and re-layouts  8.14 us (6%)
    pallas_call x1, Pallas kernels, on_device(): pl.pallas_call(functools.partial(whole_kernel, cfg), out_shape=(jax.Shape...  128 us
    unnamed x5, local copies, waits for them, and re-layouts  8.14 us

profile of v1, /device:TPU:0, one launch (start us, length us, event | category | flops | bytes accessed | tf_op | source)
XLA Modules:
  0.0 137.0 jit_solution(1786369121684440517)
XLA Ops:
  0.6 1.4 %copy.24.sel_ref = s32[128,2]{1,0:T(8,128)} copy(s32[128,2]{0,1:T(2,128)} %param.34) | data formatting | bytes 2048 | tf_op args[13]
  2.0 1.4 %copy.25.fac_ref = f32[128,2]{1,0:T(8,128)} copy(f32[128,2]{0,1:T(2,128)} %param.35) | data formatting | bytes 2048 | tf_op args[14]
  3.5 1.6 %copy.23.extra_ref = f32[512,8]{1,0:T(8,128)} copy(f32[512,8]{0,1:T(8,128)} %param.29) | data formatting | bytes 32768 | tf_op args[8]
  5.0 128.2 %whole.1 = (bf16[128,2048]{1,0:T(8,128)(2,1)}, bf16[128,2048]{1,0:T(8,128)(2,1)}) custom-call(bf16[512,512]{1,0:T(8,128)(2,1)} %q_ref.1, bf16[512,512]{1,0:T(8,128)(2,1)} %k_ref.1, bf16[512,512]{1,0:T(8,128)(2,1)} %v_ref.1, bf16[512,512]{1,0:T(8,128)(2,1)} %f_ref.1, bf16[512,512]{1,0:T(8,128)(2,1)} %a_ref.1, f32[1,512]{1,0:T(1,128)} %bitcast.11, ...), custom_call_target="tpu_custom_call" | custom-call | tf_op jit(solution)/shard_map/whole/pallas_call | solution.py:997
  133.2 1.9 %copy.28 = bf16[128,2048]{1,0:T(8,128)(2,1)} copy(bf16[128,2048]{1,0:T(8,128)(2,1)} %get-tuple-element.4) | data formatting | bytes 1048576
  135.1 1.9 %copy.29 = bf16[128,2048]{1,0:T(8,128)(2,1)} copy(bf16[128,2048]{1,0:T(8,128)(2,1)} %get-tuple-element.5) | data formatting | bytes 1048576

commit v2 on v1

--- a/solution.py
+++ b/solution.py
@@ -481,32 +481,33 @@
     gate_hbm, map_hbm, gw_hbm, uw_hbm, dw_hbm, cg_hbm, cu_hbm, cd_hbm,
     mix_out, moe_out,
     xg, wg, flat, memory, parts, state, mixed, mp, mc, mx,
-    part, rc, rx, zb, tb, acc,
+    part, rc, zb, acc, extra_v,
     gate_v, map_v, gw_v, uw_v, dw_v, cg_v, cu_v, cd_v,
     local_sem,
-    agz_s, agz_r, agx_s, agx_r, agd_s, agd_r, w_s, w_r, st_s, st_r,
-    md_s, md_r, mx_s, mx_r, rd_s, rd_r, rx_s, rx_r, rz_s, rz_r,
+    agz_s, agz_r, agd_s, agd_r, w_s, w_r, st_s, st_r,
+    wx_s, wx_r, wy_s, wy_r,
+    md_s, md_r, mx_s, mx_r, rd_s, rd_r, rz_s, rz_r,
 ):
     E, T, R, heads, size, span, steps = cfg
-    X = 2
+    C = 2
+    X = T // C
     D = xg.shape[1]
     g = lax.axis_index("grp")
     e = lax.axis_index("ep")
     t = lax.axis_index("tp")
-    x = t // 2
-    c = t % 2
+    x = t // C
+    c = t % C
     f32 = jnp.float32
     bf16 = jnp.bfloat16
     last = E - 1
 
     def at(ee, xx, cc):
-        return (g, ee, 2 * xx + cc)
-
-    def block(ref, b):
-        return ref.at[pl.ds(pl.multiple_of(b * R, R), R)]
-
-    def index(ee, xx, cc):
-        return ee * T + 2 * xx + cc
+        return (g, ee, C * xx + cc)
+
+    here_dev = at(e, x, c)
+
+    def block(ref, b, rows=R):
+        return ref.at[pl.ds(pl.multiple_of(b * rows, rows), rows)]
 
     def remote(src, dst, ssem, rsem, target):
         return pltpu.make_async_remote_copy(
@@ -515,25 +516,26 @@
         )
 
     barrier = pltpu.get_barrier_semaphore()
-    for de in range(E):
-        for dt in range(T):
-            if de or dt:
-                pl.semaphore_signal(
-                    barrier, inc=1, device_id=(g, (e + de) % E, (t + dt) % T), device_id_type=MESH
-                )
+    column = [(de, dc) for de in range(E) for dc in range(C) if de or dc]
+    greeted = [((e + de) % E, (c + dc) % C) for de, dc in column]
+    for ee, cc in greeted:
+        pl.semaphore_signal(barrier, inc=1, device_id=at(ee, x, cc), device_id_type=MESH)
+    pl.semaphore_signal(barrier, inc=1, device_id=at(e, 1 - x, c), device_id_type=MESH)
+    pl.semaphore_signal(barrier, inc=1, device_id=(1 - g, e, t), device_id_type=MESH)
     locals_ = [
         pltpu.make_async_copy(a, b, local_sem.at[n])
         for n, (a, b) in enumerate(
             [
-                (gate_hbm, gate_v), (map_hbm, map_v), (gw_hbm, gw_v), (uw_hbm, uw_v),
-                (dw_hbm, dw_v), (cg_hbm, cg_v), (cu_hbm, cu_v), (cd_hbm, cd_v),
+                (gate_hbm, gate_v), (map_hbm, map_v),
+                (gw_hbm, gw_v.at[0]), (uw_hbm, uw_v.at[0]), (dw_hbm, dw_v.at[0]),
+                (cg_hbm, cg_v.at[0]), (cu_hbm, cu_v.at[0]), (cd_hbm, cd_v.at[0]),
             ]
         )
     ]
     for copy in locals_:
         copy.start()
 
-    mine = index(e, x, c)
+    mine = C * e + c
 
     @pl.loop(0, R // 16)
     def _(r):
@@ -545,53 +547,40 @@
         )
         xg[pl.ds(pl.multiple_of(mine * R + r * 16, 16), 16), :] = normed.astype(bf16)
 
-    lane = lax.broadcasted_iota(jnp.int32, (R, 128), 1)
-    weights = jnp.zeros((R, 128), f32)
-    for j in range(sel_ref.shape[1]):
-        weights = weights + jnp.where(lane == sel_ref[:, j : j + 1], fac_ref[:, j : j + 1], 0.0)
     wrows = wg.shape[1]
-    wg[mine] = weights.T[:wrows]
-    pl.semaphore_wait(barrier, E * T - 1)
+    wrow = lax.broadcasted_iota(jnp.int32, (wrows, R), 0)
+    weights = jnp.zeros((wrows, R), f32)
+    for j in range(sel_ref.shape[0]):
+        weights = weights + jnp.where(
+            wrow == sel_ref[j : j + 1, :], fac_ref[j : j + 1, :], 0.0
+        )
+    wg[mine] = weights
+    extra_v[...] = extra_ref[...].T
+    pl.semaphore_wait(barrier, len(column) + 2)
 
     def zr(k):
-        b = index(e - k, x, c)
+        b = C * (e - k) + c
         return remote(block(xg, b), block(xg, b), agz_s.at[0, k], agz_r.at[0, k], at(e + 1, x, c))
 
     def zl(k):
-        b = index(e + k, x, c)
+        b = C * (e + k) + c
         return remote(block(xg, b), block(xg, b), agz_s.at[1, k], agz_r.at[1, k], at(e - 1, x, c))
 
-    def xs(ee):
-        b = index(ee, x, c)
-        return remote(block(xg, b), block(xg, b), agx_s.at[ee], agx_r.at[ee], at(e, 1 - x, c))
-
-    def ds(ee, xx):
-        b = index(ee, xx, c)
-        n = ee * X + xx
-        return remote(block(xg, b), block(xg, b), agd_s.at[n], agd_r.at[n], at(e, x, 1 - c))
+    def ds(ee):
+        b = C * ee + c
+        return remote(block(xg, b), block(xg, b), agd_s.at[ee], agd_r.at[ee], at(e, x, 1 - c))
 
     def zr_wait(k):
-        b = index(e - 1 - k, x, c)
-        remote(block(xg, b), block(xg, b), agz_s.at[0, k], agz_r.at[0, k], at(e, x, c)).wait_recv()
+        b = C * (e - 1 - k) + c
+        remote(block(xg, b), block(xg, b), agz_s.at[0, k], agz_r.at[0, k], here_dev).wait_recv()
 
     def zl_wait(k):
-        b = index(e + 1 + k, x, c)
-        remote(block(xg, b), block(xg, b), agz_s.at[1, k], agz_r.at[1, k], at(e, x, c)).wait_recv()
-
-    def xs_wait(ee):
-        b = index(ee, 1 - x, c)
-        remote(block(xg, b), block(xg, b), agx_s.at[ee], agx_r.at[ee], at(e, x, c)).wait_recv()
-
-    def ds_wait(ee, xx):
-        b = index(ee, xx, 1 - c)
-        n = ee * X + xx
-        remote(block(xg, b), block(xg, b), agd_s.at[n], agd_r.at[n], at(e, x, c)).wait_recv()
-
-    def gather_start():
-        pl.when(e < last)(lambda: zr(0).start())
-        pl.when(e > 0)(lambda: zl(0).start())
-        xs(e).start()
-        ds(e, x).start()
+        b = C * (e + 1 + k) + c
+        remote(block(xg, b), block(xg, b), agz_s.at[1, k], agz_r.at[1, k], here_dev).wait_recv()
+
+    def ds_wait(ee):
+        b = C * ee + 1 - c
+        remote(block(xg, b), block(xg, b), agd_s.at[ee], agd_r.at[ee], here_dev).wait_recv()
 
     def gather_z(k):
         @pl.when(e >= k + 1)
@@ -599,56 +588,68 @@
             zr_wait(k)
             if k + 1 < last:
                 pl.when(e < last)(lambda: zr(k + 1).start())
-            xs(e - 1 - k).start()
-            ds(e - 1 - k, x).start()
+            ds(e - 1 - k).start()
 
         @pl.when(e + 1 + k <= last)
         def _():
             zl_wait(k)
             if k + 1 < last:
                 pl.when(e > 0)(lambda: zl(k + 1).start())
-            xs(e + 1 + k).start()
-            ds(e + 1 + k, x).start()
-
-    def gather_x(k):
-        if k == 0:
-            xs_wait(e)
-            ds(e, 1 - x).start()
-        else:
-            @pl.when(e >= k)
-            def _():
-                xs_wait(e - k)
-                ds(e - k, 1 - x).start()
-
-            @pl.when(e + k <= last)
-            def _():
-                xs_wait(e + k)
-                ds(e + k, 1 - x).start()
-
-    def gather_sends_done():
-        for k in range(last):
-            pl.when((e < last) & (e >= k))(lambda: zr(k).wait_send())
-            pl.when((e > 0) & (e + k <= last))(lambda: zl(k).wait_send())
-        for ee in range(E):
-            xs(ee).wait_send()
-            for xx in range(X):
-                ds(ee, xx).wait_send()
-
-    def w_copy(de, dt):
-        n = de * T + dt - 1
+            ds(e + 1 + k).start()
+
+    def w_copy(n):
+        ee, cc = greeted[n]
+        return remote(wg.at[mine], wg.at[mine], w_s.at[n], w_r.at[n], at(ee, x, cc))
+
+    def w_wait(n):
+        de, dc = column[n]
+        b = C * ((e - de + E) % E) + (c - dc + C) % C
+        remote(wg.at[b], wg.at[b], w_s.at[n], w_r.at[n], here_dev).wait_recv()
+
+    pieces = []
+    for src, dst, cuts in (
+        (gw_hbm, gw_v, 2), (uw_hbm, uw_v, 2), (dw_hbm, dw_v, 2),
+        (cg_hbm, cg_v, 1), (cu_hbm, cu_v, 1), (cd_hbm, cd_v, 1),
+    ):
+        rows = src.shape[0] // (2 * cuts)
+        for n in range(cuts):
+            pieces.append((src, dst, rows, cuts, n))
+
+    def wx(p):
+        src, dst, rows, cuts, n = pieces[p]
+        b = g * cuts + n
         return remote(
-            wg.at[mine], wg.at[mine], w_s.at[n], w_r.at[n], (g, (e + de) % E, (t + dt) % T)
-        )
-
-    def w_wait(de, dt):
-        n = de * T + dt - 1
-        b = ((e - de + E) % E) * T + (t - dt + T) % T
-        remote(wg.at[b], wg.at[b], w_s.at[n], w_r.at[n], at(e, x, c)).wait_recv()
-
-    others = [(de, dt) for de in range(E) for dt in range(T) if de or dt]
-    gather_start()
-    for de, dt in others:
-        w_copy(de, dt).start()
+            block(src, b, rows), block(dst.at[1], b, rows), wx_s.at[p], wx_r.at[p],
+            at(e, 1 - x, c),
+        )
+
+    def wy(p):
+        src, dst, rows, cuts, n = pieces[p]
+        b = g * cuts + n
+        return remote(
+            block(dst.at[1], b, rows), block(dst.at[1], b, rows), wy_s.at[p], wy_r.at[p],
+            (1 - g, e, t),
+        )
+
+    def wy_wait(p):
+        src, dst, rows, cuts, n = pieces[p]
+        b = (1 - g) * cuts + n
+        remote(
+            block(dst.at[1], b, rows), block(dst.at[1], b, rows), wy_s.at[p], wy_r.at[p],
+            here_dev,
+        ).wait_recv()
+
+    def pass_on(p):
+        wx(p).wait_recv()
+        wy(p).start()
+
+    pl.when(e < last)(lambda: zr(0).start())
+    pl.when(e > 0)(lambda: zl(0).start())
+    for p in range(len(pieces)):
+        wx(p).start()
+    ds(e).start()
+    for n in range(len(column)):
+        w_copy(n).start()
 
     mrow = lax.broadcasted_iota(jnp.int32, (2 * size, size), 0)
     mcol = lax.broadcasted_iota(jnp.int32, (2 * size, size), 1)
@@ -656,18 +657,25 @@
     for h in range(heads):
         memory[h] = begin
 
-    hop_at = [max(1, (3 * steps) // 8), max(1, (6 * steps) // 8)]
+    def during(part_of):
+        return min(steps - 1, (part_of * steps) // 8)
+
+    hops = [(during(3), gather_z, 0), (during(6), gather_z, 1)]
+    hops = [hop for hop in hops if hop[2] < last]
+    hops += [(during(2), pass_on, 0), (during(3), pass_on, 1), (during(5), pass_on, 2),
+             (during(6), pass_on, 3)]
+    early = len([hop for hop in hops if hop[1] is gather_z])
 
     @pl.loop(0, steps)
     def _(i):
-        for n, when in enumerate(hop_at):
-            if n < last:
-                @pl.when(i == when)
-                def _():
-                    gather_z(n)
-                    gather_x(n)
+        for when in sorted({hop[0] for hop in hops}):
+            @pl.when(i == when)
+            def _():
+                for step, act, n in hops:
+                    if step == when:
+                        act(n)
         span_step(
-            heads, size, span, i, q_ref, k_ref, v_ref, f_ref, a_ref, fb_ref, ab_ref, extra_ref,
+            heads, size, span, i, q_ref, k_ref, v_ref, f_ref, a_ref, fb_ref, ab_ref, extra_v,
             flat, memory,
         )
 
@@ -679,11 +687,13 @@
 
     def st_wait(d):
         k = e - d
-        remote(parts.at[k], parts.at[k], st_s.at[d - 1], st_r.at[d - 1], at(e, x, c)).wait_recv()
+        remote(parts.at[k], parts.at[k], st_s.at[d - 1], st_r.at[d - 1], here_dev).wait_recv()
 
     for d in range(1, E):
         pl.when(e + d <= last)(lambda: st_copy(d).start())
-    for k in range(len(hop_at), last):
+    pass_on(4)
+    pass_on(5)
+    for k in range(early, last):
         gather_z(k)
     state[...] = jnp.zeros_like(state)
     for d in range(1, E):
@@ -716,34 +726,29 @@
         gate = jax.nn.sigmoid(gate_v[here, :].astype(f32))
         mixed[here, :] = (scaled * gate).astype(bf16)
 
-    for k in range(len(hop_at), E):
-        gather_x(k)
+    pass_on(6)
 
     locals_[1].wait()
 
     def md_copy(xx):
-        n = 2 * xx + 1 - c
+        n = C * xx + 1 - c
         return remote(block(mp, n), block(mc, xx), md_s.at[xx], md_r.at[xx], at(e, x, 1 - c))
 
     def mx_copy():
-        n = 2 * (1 - x) + c
+        n = C * (1 - x) + c
         return remote(block(mp, n), mx, mx_s.at[0], mx_r.at[0], at(e, 1 - x, c))
 
-    def mixer_rows(n):
-        rows = mixed[pl.ds(pl.multiple_of(n * R, R), R), :]
+    @pl.loop(0, T)
+    def _(n):
+        order = jnp.where(n < X, C * n + 1 - c, C * (n - X) + c)
+        here = pl.ds(pl.multiple_of(order * R, R), R)
+        rows = mixed[here, :]
         for j in range(D // 512):
             cols = slice(512 * j, 512 * (j + 1))
-            mp[pl.ds(pl.multiple_of(n * R, R), R), cols] = jnp.dot(
-                rows, map_v[:, cols], preferred_element_type=f32
-            ).astype(bf16)
-
-    @pl.loop(0, T)
-    def _(n):
-        order = jnp.where(n < X, 2 * n + 1 - c, 2 * (n - X) + c)
-        mixer_rows(order)
-
-    def add_rows(dst, terms, limit=16):
-        @pl.loop(0, R // limit)
+            mp[here, cols] = jnp.dot(rows, map_v[:, cols], preferred_element_type=f32).astype(bf16)
+
+    def add_rows(dst, terms, rows=R, limit=16):
+        @pl.loop(0, rows // limit)
         def _(r):
             here = pl.ds(pl.multiple_of(r * limit, limit), limit)
             total = terms[0][here, :].astype(f32)
@@ -755,149 +760,142 @@
         md_copy(xx).start()
     for xx in range(X):
         md_copy(xx).wait_recv()
-    away = block(mp, 2 * (1 - x) + c)
+    away = block(mp, C * (1 - x) + c)
     add_rows(away, [away, block(mc, 1 - x)])
     mx_copy().start()
 
     for copy in locals_[2:]:
         copy.wait()
     for ee in range(E):
-        for xx in range(X):
-            ds_wait(ee, xx)
-    for de, dt in others:
-        w_wait(de, dt)
-
-    def rd_copy(dest, xx):
-        n = dest * X + xx
+        ds_wait(ee)
+    for n in range(len(column)):
+        w_wait(n)
+    for p in range(6):
+        wy_wait(p)
+
+    def rd_copy(dest):
         return remote(
-            block(part, index(dest, xx, 1 - c)), block(rc, n), rd_s.at[n], rd_r.at[n],
+            block(part, C * dest + 1 - c), block(rc, dest), rd_s.at[dest], rd_r.at[dest],
             at(e, x, 1 - c),
-        )
-
-    def rx_copy(dest):
-        return remote(
-            block(part, index(dest, 1 - x, c)), block(rx, dest), rx_s.at[dest], rx_r.at[dest],
-            at(e, 1 - x, c),
         )
 
     def expert_rows(dest, own):
         wlane = lax.broadcasted_iota(jnp.int32, (R, wrows), 1)
-
-        @pl.loop(0, T // 2)
-        def _(half):
-            base = pl.multiple_of(dest * (T * R) + half * (2 * R), 2 * R)
-            rows = xg[pl.ds(base, 2 * R), :]
-            picked = []
-            for j in range(2):
-                table = wg[dest * T + half * 2 + j].T
-                picked.append(jnp.sum(jnp.where(wlane == e, table, 0.0), axis=1, keepdims=True))
-            column = jnp.concatenate(picked, axis=0)
-            gate_vals = jnp.dot(rows, gw_v[...], preferred_element_type=f32)
-            up_vals = jnp.dot(rows, uw_v[...], preferred_element_type=f32)
-            hidden = (jax.nn.silu(gate_vals) * up_vals * column).astype(bf16)
-            if own:
-                sg = jnp.dot(rows, cg_v[...], preferred_element_type=f32)
-                su = jnp.dot(rows, cu_v[...], preferred_element_type=f32)
-                shared = (jax.nn.silu(sg) * su).astype(bf16)
-            for j in range(D // 256):
-                cols = slice(256 * j, 256 * (j + 1))
-                total = jnp.dot(hidden, dw_v[:, cols], preferred_element_type=f32)
-                if own:
-                    total = total + jnp.dot(shared, cd_v[:, cols], preferred_element_type=f32)
-                part[pl.ds(base, 2 * R), cols] = total.astype(bf16)
+        base = pl.multiple_of(dest * (C * R), C * R)
+        rows = xg[pl.ds(base, C * R), :]
+        picked = []
+        for j in range(C):
+            table = wg[dest * C + j].T
+            picked.append(jnp.sum(jnp.where(wlane == e, table, 0.0), axis=1, keepdims=True))
+        scale = jnp.concatenate(picked, axis=0)
+        hidden = []
+        for n in range(X):
+            gate_vals = jnp.dot(rows, gw_v[n], preferred_element_type=f32)
+            up_vals = jnp.dot(rows, uw_v[n], preferred_element_type=f32)
+            hidden.append(((jax.nn.silu(gate_vals) * up_vals * scale).astype(bf16), dw_v.at[n]))
+        if own:
+            for n in range(X):
+                sg = jnp.dot(rows, cg_v[n], preferred_element_type=f32)
+                su = jnp.dot(rows, cu_v[n], preferred_element_type=f32)
+                hidden.append(((jax.nn.silu(sg) * su).astype(bf16), cd_v.at[n]))
+        for j in range(D // 256):
+            cols = slice(256 * j, 256 * (j + 1))
+            total = None
+            for left, right in hidden:
+                term = jnp.dot(left, right[:, cols], preferred_element_type=f32)
+                total = term if total is None else total + term
+            part[pl.ds(base, C * R), cols] = total.astype(bf16)
 
     def dest_of(k):
         low = jnp.where(k < last - e, last - k, k - (last - e))
         high = jnp.where(k < e, k, last - (k - e))
         return jnp.where(k == last, e, jnp.where(e < E // 2, low, high))
 
-    def fold_core(dest):
-        rd_copy(dest, 1 - x).wait_recv()
-        there = block(part, index(dest, 1 - x, c))
-        add_rows(there, [there, block(rc, dest * X + 1 - x)])
-        rx_copy(dest).start()
+    H = R // 2
+    edge = (e == 0) | (e == last)
+
+    def z_copy(dest, half):
+        up = jnp.where(dest > e, 1, 0)
+        n = up * E + dest
+        return remote(
+            block(part, (C * dest + c) * 2 + half, H), block(zb, n * 2 + half, H),
+            rz_s.at[n, half], rz_r.at[n, half], at(e + 2 * up - 1, x, c),
+        )
+
+    def z_step(dest, has_prev):
+        up = jnp.where(dest > e, 1, 0)
+        rd_copy(dest).wait_recv()
+        for half in range(2):
+            there = block(part, (C * dest + c) * 2 + half, H)
+            terms = [there, block(rc, dest * 2 + half, H)]
+            copy = z_copy(dest, half)
+            if has_prev:
+                copy.wait_recv()
+                terms.append(block(zb, (up * E + dest) * 2 + half, H))
+            add_rows(there, terms, H)
+            copy.start()
 
     @pl.loop(0, last)
     def _(k):
         dest = dest_of(k)
         expert_rows(dest, False)
-        for xx in range(X):
-            rd_copy(dest, xx).start()
-
-        @pl.when(k > 0)
+        rd_copy(dest).start()
+
+        @pl.when(edge & (k > 0))
         def _():
-            fold_core(dest_of(k - 1))
-
+            z_step(dest_of(k - 1), False)
+
+    pl.when(edge)(lambda: z_step(dest_of(last - 1), False))
+    for p in range(7, len(pieces)):
+        pass_on(p)
+    for p in range(6, len(pieces)):
+        wy_wait(p)
     expert_rows(e, True)
-    for xx in range(X):
-        rd_copy(e, xx).start()
-    fold_core(dest_of(last - 1))
-    fold_core(e)
-
-    def z_step(k):
-        dest = dest_of(k)
-        up = jnp.where(dest > e, 1, 0)
-        n = up * E + dest
-        has_prev = jnp.where(dest > e, e > 0, e < last)
-        copy = remote(
-            block(tb, dest), block(zb, n), rz_s.at[n], rz_r.at[n], at(e + 2 * up - 1, x, c)
-        )
-        rd_copy(dest, x).wait_recv()
-        rx_copy(dest).wait_recv()
-        terms = [block(part, index(dest, x, c)), block(rc, dest * X + x), block(rx, dest)]
-
-        @pl.when(has_prev)
-        def _():
-            copy.wait_recv()
-            add_rows(block(tb, dest), terms + [block(zb, n)])
-
-        @pl.when(jnp.logical_not(has_prev))
-        def _():
-            add_rows(block(tb, dest), terms)
-
-        copy.start()
-
-    pl.loop(0, last)(z_step)
+    rd_copy(e).start()
+
+    @pl.when(jnp.logical_not(edge))
+    def _():
+        @pl.loop(0, last)
+        def _(k):
+            z_step(dest_of(k), True)
 
     mx_copy().wait_recv()
-    add_rows(mix_out, [block(mp, 2 * x + c), block(mc, x), mx])
-    rd_copy(e, x).wait_recv()
-    rx_copy(e).wait_recv()
-    add_rows(acc, [block(part, index(e, x, c)), block(rc, e * X + x), block(rx, e)])
+    add_rows(mix_out, [block(mp, C * x + c), block(mc, x), mx])
+    rd_copy(e).wait_recv()
+    add_rows(acc, [block(part, C * e + c), block(rc, e)])
     for up in range(2):
-        n = up * E + e
-        copy = remote(block(tb, e), block(zb, n), rz_s.at[n], rz_r.at[n], at(e, x, c))
-
         @pl.when(e > 0 if up else e < last)
         def _():
-            copy.wait_recv()
-            add_rows(acc, [acc, block(zb, n)])
+            n = up * E + e
+            for half in range(2):
+                there = block(zb, n * 2 + half, H)
+                remote(there, there, rz_s.at[n, half], rz_r.at[n, half], here_dev).wait_recv()
+                add_rows(block(acc, half, H), [block(acc, half, H), there], H)
 
     add_rows(moe_out, [acc])
 
-    gather_sends_done()
-    for de, dt in others:
-        w_copy(de, dt).wait_send()
+    for k in range(last):
+        pl.when((e < last) & (e >= k))(lambda: zr(k).wait_send())
+        pl.when((e > 0) & (e + k <= last))(lambda: zl(k).wait_send())
+    for ee in range(E):
+        ds(ee).wait_send()
+    for n in range(len(column)):
+        w_copy(n).wait_send()
+    for p in range(len(pieces)):
+        wx(p).wait_send()
+        wy(p).wait_send()
     for d in range(1, E):
         pl.when(e + d <= last)(lambda: st_copy(d).wait_send())
     for xx in range(X):
         md_copy(xx).wait_send()
     mx_copy().wait_send()
-
-    @pl.loop(0, E)
-    def _(dest):
-        for xx in range(X):
-            rd_copy(dest, xx).wait_send()
-        rx_copy(dest).wait_send()
+    for dest in range(E):
+        rd_copy(dest).wait_send()
 
     @pl.loop(0, last)
     def _(k):
-        dest = dest_of(k)
-        up = jnp.where(dest > e, 1, 0)
-        n = up * E + dest
-        remote(
-            block(tb, dest), block(zb, n), rz_s.at[n], rz_r.at[n], at(e + 2 * up - 1, x, c)
-        ).wait_send()
+        for half in range(2):
+            z_copy(dest_of(k), half).wait_send()
 
 
 def on_device(
@@ -933,7 +931,7 @@
     ff = dispatched_switch_matrix.shape[2]
     sff = common_switch_matrix.shape[1]
     gathered = E * T * R * D * 2
-    if T != 4 or gathered > 12_000_000 or tokens != T * R or E < 2:
+    if T != 4 or lax.axis_size("grp") != 2 or gathered > 12_000_000 or tokens != T * R or E < 2:
         return collective_plan(
             query_vectors,
             attend_lookup_vectors,
@@ -964,8 +962,8 @@
     vmem = pl.BlockSpec(memory_space=pltpu.VMEM)
     hbm = pl.BlockSpec(memory_space=pl.ANY)
     scratch = [
-        pltpu.VMEM((E * T * R, D), bf16),
-        pltpu.VMEM((E * T, wrows, R), f32),
+        pltpu.VMEM((E * 2 * R, D), bf16),
+        pltpu.VMEM((E * 2, wrows, R), f32),
         pltpu.VMEM((tokens, 2 * mix_width), f32),
         pltpu.VMEM((heads, 2 * size, size), f32),
         pltpu.VMEM((E, heads, size, 2 * size), bf16),
@@ -974,25 +972,25 @@
         pltpu.VMEM((T * R, D), bf16),
         pltpu.VMEM((2 * R, D), bf16),
         pltpu.VMEM((R, D), bf16),
-        pltpu.VMEM((E * T * R, D), bf16),
         pltpu.VMEM((E * 2 * R, D), bf16),
         pltpu.VMEM((E * R, D), bf16),
         pltpu.VMEM((2 * E * R, D), bf16),
-        pltpu.VMEM((E * R, D), bf16),
         pltpu.VMEM((R, D), f32),
+        pltpu.VMEM((tokens, heads), f32),
         pltpu.VMEM((tokens, mix_width), bf16),
         pltpu.VMEM((mix_width, D), bf16),
-        pltpu.VMEM((D, ff), bf16),
-        pltpu.VMEM((D, ff), bf16),
-        pltpu.VMEM((ff, D), bf16),
-        pltpu.VMEM((D, sff), bf16),
-        pltpu.VMEM((D, sff), bf16),
-        pltpu.VMEM((sff, D), bf16),
+        pltpu.VMEM((2, D, ff), bf16),
+        pltpu.VMEM((2, D, ff), bf16),
+        pltpu.VMEM((2, ff, D), bf16),
+        pltpu.VMEM((2, D, sff), bf16),
+        pltpu.VMEM((2, D, sff), bf16),
+        pltpu.VMEM((2, sff, D), bf16),
         dma((8,)),
         dma((2, E)), dma((2, E)), dma((E,)), dma((E,)), dma((2 * E,)), dma((2 * E,)),
-        dma((E * T,)), dma((E * T,)), dma((E,)), dma((E,)),
+        dma((E,)), dma((E,)),
+        dma((9,)), dma((9,)), dma((9,)), dma((9,)),
         dma((2,)), dma((2,)), dma((1,)), dma((1,)),
-        dma((2 * E,)), dma((2 * E,)), dma((E,)), dma((E,)), dma((2 * E,)), dma((2 * E,)),
+        dma((E,)), dma((E,)), dma((2 * E, 2)), dma((2 * E, 2)),
     ]
     return pl.pallas_call(
         functools.partial(whole_kernel, cfg),
@@ -1015,12 +1013,12 @@
         amend_speed_dependent,
         feature_forget_baseline.reshape(1, mix_width),
         amend_speed_baseline.reshape(1, mix_width),
-        sudden_forget_extra,
+        sudden_forget_extra.T,
         group_scaling_factor.reshape(1, mix_width),
         specialist_tokens_activations,
         specialist_scaling_factor.reshape(1, D),
-        selected_specialists,
-        selection_mixing_factors,
+        selected_specialists.T,
+        selection_mixing_factors.T,
         result_switch_preactivation,
         result_mapping_matrix,
         dispatched_switch_matrix.reshape(D, ff),

time: 139 us -> 112 us (0.81)
  the two profiles are of different devices: /device:TPU:0 before, /device:TPU:9 now
where the time goes in v2:
time: 112 us
  Pallas kernels  107 us (96%)
  local copies, waits for them, and re-layouts  3.76 us (3%)
    pallas_call x1, Pallas kernels, on_device(): pl.pallas_call(functools.partial(whole_kernel, cfg), out_shape=(jax.Shape...  107 us
    unnamed x2, local copies, waits for them, and re-layouts  3.76 us

profile of v2, /device:TPU:9, one launch (start us, length us, event | category | flops | bytes accessed | tf_op | source)
XLA Modules:
  0.0 111.5 jit_solution(8025974618458039530)
XLA Ops:
  0.6 107.1 %whole.1 = (bf16[128,2048]{1,0:T(8,128)(2,1)}, bf16[128,2048]{1,0:T(8,128)(2,1)}) custom-call(bf16[512,512]{1,0:T(8,128)(2,1)} %q_ref.1, bf16[512,512]{1,0:T(8,128)(2,1)} %k_ref.1, bf16[512,512]{1,0:T(8,128)(2,1)} %v_ref.1, bf16[512,512]{1,0:T(8,128)(2,1)} %f_ref.1, bf16[512,512]{1,0:T(8,128)(2,1)} %a_ref.1, f32[1,512]{1,0:T(1,128)} %bitcast.15, ...), custom_call_target="tpu_custom_call" | custom-call | tf_op jit(solution)/shard_map/whole/pallas_call | solution.py:995
  107.8 1.9 %copy.25 = bf16[128,2048]{1,0:T(8,128)(2,1)} copy(bf16[128,2048]{1,0:T(8,128)(2,1)} %get-tuple-element.4) | data formatting | bytes 1048576
  109.6 1.9 %copy.26 = bf16[128,2048]{1,0:T(8,128)(2,1)} copy(bf16[128,2048]{1,0:T(8,128)(2,1)} %get-tuple-element.5) | data formatting | bytes 1048576

commit v3 on v2

--- a/solution.py
+++ b/solution.py
@@ -476,19 +476,20 @@
 
 def whole_kernel(
     cfg,
-    q_ref, k_ref, v_ref, f_ref, a_ref, fb_ref, ab_ref, extra_ref, gain_ref,
-    tok_ref, scale_ref, sel_ref, fac_ref,
+    fb_ref, ab_ref, extra_ref, gain_ref, scale_ref, sel_ref, fac_ref,
+    tok_hbm, q_hbm, k_hbm, v_hbm, f_hbm, a_hbm,
     gate_hbm, map_hbm, gw_hbm, uw_hbm, dw_hbm, cg_hbm, cu_hbm, cd_hbm,
     mix_out, moe_out,
     xg, wg, flat, memory, parts, state, mixed, mp, mc, mx,
-    part, rc, zb, acc, extra_v,
+    part, rc, zb, extra_v, hid, hall, hpack,
+    tok_ref, q_ref, k_ref, v_ref, f_ref, a_ref,
     gate_v, map_v, gw_v, uw_v, dw_v, cg_v, cu_v, cd_v,
     local_sem,
     agz_s, agz_r, agd_s, agd_r, w_s, w_r, st_s, st_r,
     wx_s, wx_r, wy_s, wy_r,
     md_s, md_r, mx_s, mx_r, rd_s, rd_r, rz_s, rz_r,
 ):
-    E, T, R, heads, size, span, steps = cfg
+    E, T, R, heads, size, span, steps, cap = cfg
     C = 2
     X = T // C
     D = xg.shape[1]
@@ -526,7 +527,8 @@
         pltpu.make_async_copy(a, b, local_sem.at[n])
         for n, (a, b) in enumerate(
             [
-                (gate_hbm, gate_v), (map_hbm, map_v),
+                (tok_hbm, tok_ref), (q_hbm, q_ref), (k_hbm, k_ref), (v_hbm, v_ref),
+                (f_hbm, f_ref), (a_hbm, a_ref), (gate_hbm, gate_v), (map_hbm, map_v),
                 (gw_hbm, gw_v.at[0]), (uw_hbm, uw_v.at[0]), (dw_hbm, dw_v.at[0]),
                 (cg_hbm, cg_v.at[0]), (cu_hbm, cu_v.at[0]), (cd_hbm, cd_v.at[0]),
             ]
@@ -536,6 +538,102 @@
         copy.start()
 
     mine = C * e + c
+
+    def zr(k):
+        b = C * (e - k) + c
+        return remote(block(xg, b), block(xg, b), agz_s.at[0, k], agz_r.at[0, k], at(e + 1, x, c))
+
+    def zl(k):
+        b = C * (e + k) + c
+        return remote(block(xg, b), block(xg, b), agz_s.at[1, k], agz_r.at[1, k], at(e - 1, x, c))
+
+    def ds(ee):
+        b = C * ee + c
+        return remote(block(xg, b), block(xg, b), agd_s.at[ee], agd_r.at[ee], at(e, x, 1 - c))
+
+    def zr_wait(k):
+        b = C * (e - 1 - k) + c
+        remote(block(xg, b), block(xg, b), agz_s.at[0, k], agz_r.at[0, k], here_dev).wait_recv()
+
+    def zl_wait(k):
+        b = C * (e + 1 + k) + c
+        remote(block(xg, b), block(xg, b), agz_s.at[1, k], agz_r.at[1, k], here_dev).wait_recv()
+
+    def ds_wait(ee):
+        b = C * ee + 1 - c
+        remote(block(xg, b), block(xg, b), agd_s.at[ee], agd_r.at[ee], here_dev).wait_recv()
+
+    def gather_z(k):
+        @pl.when(e >= k + 1)
+        def _():
+            zr_wait(k)
+            if k + 1 < last:
+                pl.when(e < last)(lambda: zr(k + 1).start())
+            ds(e - 1 - k).start()
+
+        @pl.when(e + 1 + k <= last)
+        def _():
+            zl_wait(k)
+            if k + 1 < last:
+                pl.when(e > 0)(lambda: zl(k + 1).start())
+            ds(e + 1 + k).start()
+
+    def w_copy(n):
+        ee, cc = greeted[n]
+        return remote(wg.at[mine], wg.at[mine], w_s.at[n], w_r.at[n], at(ee, x, cc))
+
+    def w_wait(n):
+        de, dc = column[n]
+        b = C * ((e - de + E) % E) + (c - dc + C) % C
+        remote(wg.at[b], wg.at[b], w_s.at[n], w_r.at[n], here_dev).wait_recv()
+
+    def by_rows(cuts, n):
+        def view(ref, gg):
+            rows = ref.shape[0] // (2 * cuts)
+            return block(ref, gg * cuts + n, rows)
+
+        return view
+
+    def by_cols(n, flip):
+        def view(ref, gg):
+            cols = ref.shape[1] // 4
+            unit = 2 * n + (1 - gg if flip else gg)
+            return ref.at[:, pl.ds(pl.multiple_of(unit * cols, cols), cols)]
+
+        return view
+
+    pieces = [
+        (gw_hbm, gw_v, by_rows(2, 0)), (gw_hbm, gw_v, by_rows(2, 1)),
+        (uw_hbm, uw_v, by_rows(2, 0)), (uw_hbm, uw_v, by_rows(2, 1)),
+        (dw_hbm, dw_v, by_cols(0, False)), (dw_hbm, dw_v, by_cols(1, False)),
+        (dw_hbm, dw_v, by_cols(1, True)),
+        (cg_hbm, cg_v, by_rows(1, 0)), (cu_hbm, cu_v, by_rows(1, 0)),
+        (cd_hbm, cd_v, by_rows(1, 0)),
+    ]
+    handed = (0, 1, 2, 3, 4, 7, 8, 9)
+
+    def wx(p):
+        src, dst, view = pieces[p]
+        return remote(
+            view(src, g), view(dst.at[1], g), wx_s.at[p], wx_r.at[p], at(e, 1 - x, c)
+        )
+
+    def wy(p, gg=g):
+        src, dst, view = pieces[p]
+        there = view(dst.at[1], gg)
+        return remote(there, there, wy_s.at[p], wy_r.at[p], (1 - g, e, t))
+
+    def wy_wait(p):
+        wy(p, 1 - g).wait_recv()
+
+    def pass_on(p):
+        wx(p).wait_recv()
+        wy(p).start()
+
+    pl.semaphore_wait(barrier, len(column) + 2)
+    for p in range(len(pieces)):
+        wx(p).start()
+    locals_[0].wait()
 
     @pl.loop(0, R // 16)
     def _(r):
@@ -556,100 +654,13 @@
         )
     wg[mine] = weights
     extra_v[...] = extra_ref[...].T
-    pl.semaphore_wait(barrier, len(column) + 2)
-
-    def zr(k):
-        b = C * (e - k) + c
-        return remote(block(xg, b), block(xg, b), agz_s.at[0, k], agz_r.at[0, k], at(e + 1, x, c))
-
-    def zl(k):
-        b = C * (e + k) + c
-        return remote(block(xg, b), block(xg, b), agz_s.at[1, k], agz_r.at[1, k], at(e - 1, x, c))
-
-    def ds(ee):
-        b = C * ee + c
-        return remote(block(xg, b), block(xg, b), agd_s.at[ee], agd_r.at[ee], at(e, x, 1 - c))
-
-    def zr_wait(k):
-        b = C * (e - 1 - k) + c
-        remote(block(xg, b), block(xg, b), agz_s.at[0, k], agz_r.at[0, k], here_dev).wait_recv()
-
-    def zl_wait(k):
-        b = C * (e + 1 + k) + c
-        remote(block(xg, b), block(xg, b), agz_s.at[1, k], agz_r.at[1, k], here_dev).wait_recv()
-
-    def ds_wait(ee):
-        b = C * ee + 1 - c
-        remote(block(xg, b), block(xg, b), agd_s.at[ee], agd_r.at[ee], here_dev).wait_recv()
-
-    def gather_z(k):
-        @pl.when(e >= k + 1)
-        def _():
-            zr_wait(k)
-            if k + 1 < last:
-                pl.when(e < last)(lambda: zr(k + 1).start())
-            ds(e - 1 - k).start()
-
-        @pl.when(e + 1 + k <= last)
-        def _():
-            zl_wait(k)
-            if k + 1 < last:
-                pl.when(e > 0)(lambda: zl(k + 1).start())
-            ds(e + 1 + k).start()
-
-    def w_copy(n):
-        ee, cc = greeted[n]
-        return remote(wg.at[mine], wg.at[mine], w_s.at[n], w_r.at[n], at(ee, x, cc))
-
-    def w_wait(n):
-        de, dc = column[n]
-        b = C * ((e - de + E) % E) + (c - dc + C) % C
-        remote(wg.at[b], wg.at[b], w_s.at[n], w_r.at[n], here_dev).wait_recv()
-
-    pieces = []
-    for src, dst, cuts in (
-        (gw_hbm, gw_v, 2), (uw_hbm, uw_v, 2), (dw_hbm, dw_v, 2),
-        (cg_hbm, cg_v, 1), (cu_hbm, cu_v, 1), (cd_hbm, cd_v, 1),
-    ):
-        rows = src.shape[0] // (2 * cuts)
-        for n in range(cuts):
-            pieces.append((src, dst, rows, cuts, n))
-
-    def wx(p):
-        src, dst, rows, cuts, n = pieces[p]
-        b = g * cuts + n
-        return remote(
-            block(src, b, rows), block(dst.at[1], b, rows), wx_s.at[p], wx_r.at[p],
-            at(e, 1 - x, c),
-        )
-
-    def wy(p):
-        src, dst, rows, cuts, n = pieces[p]
-        b = g * cuts + n
-        return remote(
-            block(dst.at[1], b, rows), block(dst.at[1], b, rows), wy_s.at[p], wy_r.at[p],
-            (1 - g, e, t),
-        )
-
-    def wy_wait(p):
-        src, dst, rows, cuts, n = pieces[p]
-        b = (1 - g) * cuts + n
-        remote(
-            block(dst.at[1], b, rows), block(dst.at[1], b, rows), wy_s.at[p], wy_r.at[p],
-            here_dev,
-        ).wait_recv()
-
-    def pass_on(p):
-        wx(p).wait_recv()
-        wy(p).start()
-
     pl.when(e < last)(lambda: zr(0).start())
     pl.when(e > 0)(lambda: zl(0).start())
-    for p in range(len(pieces)):
-        wx(p).start()
     ds(e).start()
     for n in range(len(column)):
         w_copy(n).start()
+    for copy in locals_[1:6]:
+        copy.wait()
 
     mrow = lax.broadcasted_iota(jnp.int32, (2 * size, size), 0)
     mcol = lax.broadcasted_iota(jnp.int32, (2 * size, size), 1)
@@ -662,7 +673,7 @@
 
     hops = [(during(3), gather_z, 0), (during(6), gather_z, 1)]
     hops = [hop for hop in hops if hop[2] < last]
-    hops += [(during(2), pass_on, 0), (during(3), pass_on, 1), (during(5), pass_on, 2),
+    hops += [(during(2), pass_on, 0), (during(4), pass_on, 1), (during(5), pass_on, 2),
              (during(6), pass_on, 3)]
     early = len([hop for hop in hops if hop[1] is gather_z])
 
@@ -679,46 +690,41 @@
             flat, memory,
         )
 
-    for h in range(heads):
-        parts[e, h] = jnp.concatenate([memory[h, :size], memory[h, size:]], axis=1).astype(bf16)
-
-    def st_copy(d):
-        return remote(parts.at[e], parts.at[e], st_s.at[d - 1], st_r.at[d - 1], at(e + d, x, c))
-
-    def st_wait(d):
-        k = e - d
-        remote(parts.at[k], parts.at[k], st_s.at[d - 1], st_r.at[d - 1], here_dev).wait_recv()
-
-    for d in range(1, E):
-        pl.when(e + d <= last)(lambda: st_copy(d).start())
+    def st_copy():
+        return remote(parts.at[0], parts.at[1], st_s.at[0], st_r.at[0], at(e + 1, x, c))
+
+    def st_step(first):
+        if not first:
+            st_copy().wait_recv()
+        for h in range(heads):
+            after = memory[h, :size]
+            if not first:
+                before = parts[1, h]
+                carry = split_two(memory[h, size:])
+                after = after + (
+                    jnp.dot(before, carry[0], preferred_element_type=f32)
+                    + jnp.dot(before, carry[1], preferred_element_type=f32)
+                )
+            parts[0, h] = after.astype(bf16)
+        pl.when(e < last)(lambda: st_copy().start())
+
+    pl.when(e == 0)(lambda: st_step(True))
     pass_on(4)
-    pass_on(5)
     for k in range(early, last):
         gather_z(k)
-    state[...] = jnp.zeros_like(state)
-    for d in range(1, E):
-        pl.when(e >= d)(lambda: st_wait(d))
-
-    @pl.loop(0, e)
-    def _(k):
-        for h in range(heads):
-            piece = parts[k, h]
-            own = split_two(state[h])
-            carry = piece[:, size:]
-            moved = jnp.dot(own[0], carry, preferred_element_type=f32) + jnp.dot(
-                own[1], carry, preferred_element_type=f32
-            )
-            state[h] = moved + piece[:, :size].astype(f32)
-
-    locals_[0].wait()
-
-    @pl.loop(0, steps)
-    def _(i):
+    pl.when(e == 1)(lambda: st_step(False))
+
+    def finish_step(i):
         here = pl.ds(pl.multiple_of(i * span, span), span)
         centered_all = []
         for h in range(heads):
             pane = flat[here, 2 * size * h : 2 * size * (h + 1)]
-            head_out = pane[:, :size] + dot3(pane[:, size:], state[h], NT)
+            head_out = pane[:, :size]
+            left = split_two(pane[:, size:])
+            head_out = head_out + (
+                lax.dot_general(left[0], state[h], NT, preferred_element_type=f32)
+                + lax.dot_general(left[1], state[h], NT, preferred_element_type=f32)
+            )
             centered = head_out - jnp.mean(head_out, -1, keepdims=True)
             head_var = jnp.mean(centered * centered, -1, keepdims=True)
             centered_all.append(centered * lax.rsqrt(head_var + 0.00064))
@@ -726,9 +732,19 @@
         gate = jax.nn.sigmoid(gate_v[here, :].astype(f32))
         mixed[here, :] = (scaled * gate).astype(bf16)
 
-    pass_on(6)
-
-    locals_[1].wait()
+    def finish():
+        locals_[6].wait()
+
+        @pl.when(e == 0)
+        def _():
+            state[...] = jnp.zeros_like(state)
+
+        @pl.when(e > 0)
+        def _():
+            state[...] = parts[1]
+
+        pl.loop(0, steps)(finish_step)
+
 
     def md_copy(xx):
         n = C * xx + 1 - c
@@ -737,15 +753,6 @@
     def mx_copy():
         n = C * (1 - x) + c
         return remote(block(mp, n), mx, mx_s.at[0], mx_r.at[0], at(e, 1 - x, c))
-
-    @pl.loop(0, T)
-    def _(n):
-        order = jnp.where(n < X, C * n + 1 - c, C * (n - X) + c)
-        here = pl.ds(pl.multiple_of(order * R, R), R)
-        rows = mixed[here, :]
-        for j in range(D // 512):
-            cols = slice(512 * j, 512 * (j + 1))
-            mp[here, cols] = jnp.dot(rows, map_v[:, cols], preferred_element_type=f32).astype(bf16)
 
     def add_rows(dst, terms, rows=R, limit=16):
         @pl.loop(0, rows // limit)
@@ -756,123 +763,246 @@
                 total = total + term[here, :].astype(f32)
             dst[here, :] = total.astype(dst.dtype)
 
-    for xx in range(X):
-        md_copy(xx).start()
-    for xx in range(X):
-        md_copy(xx).wait_recv()
-    away = block(mp, C * (1 - x) + c)
-    add_rows(away, [away, block(mc, 1 - x)])
-    mx_copy().start()
-
-    for copy in locals_[2:]:
+    def mixer_out():
+        locals_[7].wait()
+
+        @pl.loop(0, T)
+        def _(n):
+            order = jnp.where(n < X, C * n + 1 - c, C * (n - X) + c)
+            here = pl.ds(pl.multiple_of(order * R, R), R)
+            rows = mixed[here, :]
+            for j in range(D // 512):
+                cols = slice(512 * j, 512 * (j + 1))
+                mp[here, cols] = jnp.dot(rows, map_v[:, cols], preferred_element_type=f32).astype(bf16)
+
+        for xx in range(X):
+            md_copy(xx).start()
+        for xx in range(X):
+            md_copy(xx).wait_recv()
+        away = block(mp, C * (1 - x) + c)
+        add_rows(away, [away, block(mc, 1 - x)])
+        mx_copy().start()
+
+    for copy in locals_[8:]:
         copy.wait()
     for ee in range(E):
         ds_wait(ee)
     for n in range(len(column)):
         w_wait(n)
-    for p in range(6):
+    for p in range(4):
         wy_wait(p)
 
-    def rd_copy(dest):
+    W = D // 2
+
+    def pane(ref, b, half, rows=R):
+        return ref.at[pl.ds(pl.multiple_of(b * R, R), rows), pl.ds(half * W, W)]
+
+    def rd_copy(dest, half, rows=R):
         return remote(
-            block(part, C * dest + 1 - c), block(rc, dest), rd_s.at[dest], rd_r.at[dest],
-            at(e, x, 1 - c),
-        )
-
-    def expert_rows(dest, own):
-        wlane = lax.broadcasted_iota(jnp.int32, (R, wrows), 1)
+            pane(part, C * dest + 1 - c, half, rows), pane(rc, dest, half, rows),
+            rd_s.at[dest, half], rd_r.at[dest, half], at(e, x, 1 - c),
+        )
+
+    def packing(b, ee):
+        table = wg[b]
+        lanes = lax.broadcasted_iota(jnp.int32, (wrows, R), 0)
+        here = jnp.sum(jnp.where(lanes == ee, table, 0.0), axis=0, keepdims=True)
+        named = jnp.broadcast_to(jnp.where(here != 0.0, 1.0, 0.0), (8, R))
+        r0 = lax.broadcasted_iota(jnp.int32, (R, R), 0)
+        r1 = lax.broadcasted_iota(jnp.int32, (R, R), 1)
+        upto = jnp.where(r0 <= r1, 1.0, 0.0).astype(bf16)
+        place = jnp.dot(named.astype(bf16), upto, preferred_element_type=f32)[:1] * named[:1]
+        slot = lax.broadcasted_iota(jnp.int32, (cap, R), 0) + 1
+        return jnp.where(slot.astype(f32) == place, 1.0, 0.0).astype(bf16)
+
+    def add_packed(dst, terms, b, ee, packed):
+        spread = packing(b, ee)
+        for j in range(W // 256):
+            cols = slice(256 * j, 256 * (j + 1))
+            total = lax.dot_general(
+                spread, packed[:, cols], (((0,), (0,)), ((), ())), preferred_element_type=f32
+            )
+            for term in terms:
+                total = total + term[:, cols].astype(f32)
+            dst[:, cols] = total.astype(dst.dtype)
+
+    ff = gw_v.shape[2]
+    sff = cg_v.shape[2]
+
+    def hidden_rows(dest, shared=False):
         base = pl.multiple_of(dest * (C * R), C * R)
         rows = xg[pl.ds(base, C * R), :]
+        if shared:
+            for n in range(X):
+                sg = jnp.dot(rows, cg_v[n], preferred_element_type=f32)
+                su = jnp.dot(rows, cu_v[n], preferred_element_type=f32)
+                hid[:, sff * n : sff * (n + 1)] = (jax.nn.silu(sg) * su).astype(bf16)
+            return
+        wlane = lax.broadcasted_iota(jnp.int32, (R, wrows), 1)
         picked = []
         for j in range(C):
             table = wg[dest * C + j].T
             picked.append(jnp.sum(jnp.where(wlane == e, table, 0.0), axis=1, keepdims=True))
         scale = jnp.concatenate(picked, axis=0)
-        hidden = []
         for n in range(X):
             gate_vals = jnp.dot(rows, gw_v[n], preferred_element_type=f32)
             up_vals = jnp.dot(rows, uw_v[n], preferred_element_type=f32)
-            hidden.append(((jax.nn.silu(gate_vals) * up_vals * scale).astype(bf16), dw_v.at[n]))
-        if own:
+            hall[dest, :, ff * n : ff * (n + 1)] = (
+                jax.nn.silu(gate_vals) * up_vals * scale
+            ).astype(bf16)
+
+    def pack_rows(dest):
+        for j in range(C):
+            hpack[j] = jnp.dot(
+                packing(C * dest + j, e), hall[dest, j * R : (j + 1) * R, :],
+                preferred_element_type=f32,
+            ).astype(bf16)
+        for j in range(C):
+            hall[dest, j * cap : (j + 1) * cap, :] = hpack[j]
+
+    def part_rows(dest, half, own=False, rows=R):
+        base = pl.multiple_of(dest * (C * R), C * R)
+        for j in range(W // 256):
+            cols = slice(half * W + 256 * j, half * W + 256 * (j + 1))
+            total = None
             for n in range(X):
-                sg = jnp.dot(rows, cg_v[n], preferred_element_type=f32)
-                su = jnp.dot(rows, cu_v[n], preferred_element_type=f32)
-                hidden.append(((jax.nn.silu(sg) * su).astype(bf16), cd_v.at[n]))
-        for j in range(D // 256):
-            cols = slice(256 * j, 256 * (j + 1))
-            total = None
-            for left, right in hidden:
-                term = jnp.dot(left, right[:, cols], preferred_element_type=f32)
+                term = jnp.dot(
+                    hall[dest, : C * rows, ff * n : ff * (n + 1)], dw_v[n, :, cols],
+                    preferred_element_type=f32,
+                )
                 total = term if total is None else total + term
-            part[pl.ds(base, C * R), cols] = total.astype(bf16)
+                if own:
+                    total = total + jnp.dot(
+                        hid[:, sff * n : sff * (n + 1)], cd_v[n, :, cols],
+                        preferred_element_type=f32,
+                    )
+            for i in range(C):
+                part[pl.ds(base + i * R, rows), cols] = total[i * rows : (i + 1) * rows].astype(
+                    bf16
+                )
 
     def dest_of(k):
         low = jnp.where(k < last - e, last - k, k - (last - e))
         high = jnp.where(k < e, k, last - (k - e))
         return jnp.where(k == last, e, jnp.where(e < E // 2, low, high))
 
-    H = R // 2
     edge = (e == 0) | (e == last)
 
-    def z_copy(dest, half):
+    def z_copy(dest, half, rows=R):
         up = jnp.where(dest > e, 1, 0)
         n = up * E + dest
         return remote(
-            block(part, (C * dest + c) * 2 + half, H), block(zb, n * 2 + half, H),
+            pane(part, C * dest + c, half, rows), pane(zb, n, half, rows),
             rz_s.at[n, half], rz_r.at[n, half], at(e + 2 * up - 1, x, c),
         )
 
-    def z_step(dest, has_prev):
+    def z_take(dst, terms, n, half, b, giver):
+        packed_too = (giver == 0) | (giver == last)
+
+        @pl.when(packed_too)
+        def _():
+            there = pane(zb, n, half, cap)
+            remote(there, there, rz_s.at[n, half], rz_r.at[n, half], here_dev).wait_recv()
+            add_packed(dst, terms, b, giver, there)
+
+        @pl.when(jnp.logical_not(packed_too))
+        def _():
+            there = pane(zb, n, half)
+            remote(there, there, rz_s.at[n, half], rz_r.at[n, half], here_dev).wait_recv()
+            add_rows(dst, terms + [there])
+
+    def edge_step(dest, half):
+        rd_copy(dest, half, cap).wait_recv()
+        there = pane(part, C * dest + c, half, cap)
+        add_rows(there, [there, pane(rc, dest, half, cap)], cap)
+        z_copy(dest, half, cap).start()
+
+    def middle_step(dest, half):
         up = jnp.where(dest > e, 1, 0)
-        rd_copy(dest).wait_recv()
-        for half in range(2):
-            there = block(part, (C * dest + c) * 2 + half, H)
-            terms = [there, block(rc, dest * 2 + half, H)]
-            copy = z_copy(dest, half)
-            if has_prev:
-                copy.wait_recv()
-                terms.append(block(zb, (up * E + dest) * 2 + half, H))
-            add_rows(there, terms, H)
-            copy.start()
-
-    @pl.loop(0, last)
-    def _(k):
-        dest = dest_of(k)
-        expert_rows(dest, False)
-        rd_copy(dest).start()
-
-        @pl.when(edge & (k > 0))
+        rd_copy(dest, half).wait_recv()
+        there = pane(part, C * dest + c, half)
+        z_take(
+            there, [there, pane(rc, dest, half)], up * E + dest, half, C * dest + c,
+            e + 1 - 2 * up,
+        )
+        z_copy(dest, half).start()
+
+    def experts(half):
+        @pl.when(edge)
         def _():
-            z_step(dest_of(k - 1), False)
-
-    pl.when(edge)(lambda: z_step(dest_of(last - 1), False))
-    for p in range(7, len(pieces)):
-        pass_on(p)
-    for p in range(6, len(pieces)):
+            @pl.loop(0, last)
+            def _(k):
+                dest = dest_of(k)
+                if half == 0:
+                    hidden_rows(dest)
+                    pack_rows(dest)
+
+                    @pl.when(k > 0)
+                    def _():
+                        edge_step(dest_of(k - 1), half)
+
+                part_rows(dest, half, rows=cap)
+                rd_copy(dest, half, cap).start()
+                if half:
+                    @pl.when(k > 0)
+                    def _():
+                        edge_step(dest_of(k - 1), half)
+
+            if half == 0:
+                hidden_rows(e)
+            edge_step(dest_of(last - 1), half)
+
+        @pl.when(jnp.logical_not(edge))
+        def _():
+            @pl.loop(0, last)
+            def _(k):
+                dest = dest_of(k)
+                if half == 0:
+                    hidden_rows(dest)
+                part_rows(dest, half)
+                rd_copy(dest, half).start()
+
+            if half == 0:
+                hidden_rows(e)
+
+    def middle(k, half):
+        pl.when(jnp.logical_not(edge))(lambda: middle_step(dest_of(k), half))
+
+    wy_wait(4)
+    experts(0)
+    pl.when(e == 2)(lambda: st_step(False))
+    wx(5).wait_recv()
+    wx(6).wait_recv()
+    experts(1)
+    pl.when(e > 2)(lambda: st_step(False))
+    middle(0, 0)
+    finish()
+    pass_on(7)
+    for k in range(1, last):
+        middle(k, 0)
+    mixer_out()
+    pass_on(8)
+    middle(0, 1)
+    pass_on(9)
+    for k in range(1, last):
+        middle(k, 1)
+    for p in (7, 8, 9):
         wy_wait(p)
-    expert_rows(e, True)
-    rd_copy(e).start()
-
-    @pl.when(jnp.logical_not(edge))
-    def _():
-        @pl.loop(0, last)
-        def _(k):
-            z_step(dest_of(k), True)
-
+    hidden_rows(e, True)
+    for half in range(2):
+        part_rows(e, half, True)
+        rd_copy(e, half).start()
     mx_copy().wait_recv()
     add_rows(mix_out, [block(mp, C * x + c), block(mc, x), mx])
-    rd_copy(e).wait_recv()
-    add_rows(acc, [block(part, C * e + c), block(rc, e)])
-    for up in range(2):
-        @pl.when(e > 0 if up else e < last)
-        def _():
-            n = up * E + e
-            for half in range(2):
-                there = block(zb, n * 2 + half, H)
-                remote(there, there, rz_s.at[n, half], rz_r.at[n, half], here_dev).wait_recv()
-                add_rows(block(acc, half, H), [block(acc, half, H), there], H)
-
-    add_rows(moe_out, [acc])
+
+    for half in range(2):
+        rd_copy(e, half).wait_recv()
+        out = moe_out.at[:, pl.ds(half * W, W)]
+        add_rows(out, [pane(part, C * e + c, half), pane(rc, e, half)])
+        for up in range(2):
+            @pl.when(e > 0 if up else e < last)
+            def _():
+                z_take(out, [out], up * E + e, half, C * e + c, e + 1 - 2 * up)
 
     for k in range(last):
         pl.when((e < last) & (e >= k))(lambda: zr(k).wait_send())
@@ -883,19 +1013,21 @@
         w_copy(n).wait_send()
     for p in range(len(pieces)):
         wx(p).wait_send()
+    for p in handed:
         wy(p).wait_send()
-    for d in range(1, E):
-        pl.when(e + d <= last)(lambda: st_copy(d).wait_send())
+    pl.when(e < last)(lambda: st_copy().wait_send())
     for xx in range(X):
         md_copy(xx).wait_send()
     mx_copy().wait_send()
-    for dest in range(E):
-        rd_copy(dest).wait_send()
-
-    @pl.loop(0, last)
-    def _(k):
-        for half in range(2):
-            z_copy(dest_of(k), half).wait_send()
+    for half in range(2):
+        rd_copy(e, half).wait_send()
+        for rows, mask in ((cap, edge), (R, jnp.logical_not(edge))):
+            @pl.when(mask)
+            def _():
+                @pl.loop(0, last)
+                def _(k):
+                    rd_copy(dest_of(k), half, rows).wait_send()
+                    z_copy(dest_of(k), half, rows).wait_send()
 
 
 def on_device(
@@ -955,7 +1087,9 @@
             common_raising_matrix,
             common_lowering_matrix,
         )
-    cfg = (E, T, R, heads, size, span, tokens // span)
+    named = 3 * R * selected_specialists.shape[1] // (2 * E)
+    cap = min(R, -(-named // 16) * 16)
+    cfg = (E, T, R, heads, size, span, tokens // span, cap)
     bf16, f32 = jnp.bfloat16, jnp.float32
     wrows = -(-E // 8) * 8
     dma = pltpu.SemaphoreType.DMA
@@ -966,8 +1100,8 @@
         pltpu.VMEM((E * 2, wrows, R), f32),
         pltpu.VMEM((tokens, 2 * mix_width), f32),
         pltpu.VMEM((heads, 2 * size, size), f32),
-        pltpu.VMEM((E, heads, size, 2 * size), bf16),
-        pltpu.VMEM((heads, size, size), f32),
+        pltpu.VMEM((2, heads, size, size), bf16),
+        pltpu.VMEM((heads, size, size), bf16),
         pltpu.VMEM((tokens, mix_width), bf16),
         pltpu.VMEM((T * R, D), bf16),
         pltpu.VMEM((2 * R, D), bf16),
@@ -975,8 +1109,16 @@
         pltpu.VMEM((E * 2 * R, D), bf16),
         pltpu.VMEM((E * R, D), bf16),
         pltpu.VMEM((2 * E * R, D), bf16),
-        pltpu.VMEM((R, D), f32),
         pltpu.VMEM((tokens, heads), f32),
+        pltpu.VMEM((2 * R, 2 * sff), bf16),
+        pltpu.VMEM((E, 2 * R, 2 * ff), bf16),
+        pltpu.VMEM((2, cap, 2 * ff), bf16),
+        pltpu.VMEM((R, D), bf16),
+        pltpu.VMEM((tokens, mix_width), bf16),
+        pltpu.VMEM((tokens, mix_width), bf16),
+        pltpu.VMEM((tokens, mix_width), bf16),
+        pltpu.VMEM((tokens, mix_width), bf16),
+        pltpu.VMEM((tokens, mix_width), bf16),
         pltpu.VMEM((tokens, mix_width), bf16),
         pltpu.VMEM((mix_width, D), bf16),
         pltpu.VMEM((2, D, ff), bf16),
@@ -985,20 +1127,20 @@
         pltpu.VMEM((2, D, sff), bf16),
         pltpu.VMEM((2, D, sff), bf16),
         pltpu.VMEM((2, sff, D), bf16),
-        dma((8,)),
+        dma((14,)),
         dma((2, E)), dma((2, E)), dma((E,)), dma((E,)), dma((2 * E,)), dma((2 * E,)),
-        dma((E,)), dma((E,)),
-        dma((9,)), dma((9,)), dma((9,)), dma((9,)),
+        dma((1,)), dma((1,)),
+        dma((10,)), dma((10,)), dma((10,)), dma((10,)),
         dma((2,)), dma((2,)), dma((1,)), dma((1,)),
-        dma((E,)), dma((E,)), dma((2 * E, 2)), dma((2 * E, 2)),
+        dma((E, 2)), dma((E, 2)), dma((2 * E, 2)), dma((2 * E, 2)),
     ]
-    return pl.pallas_call(
+    mix_sum, moe_sum = pl.pallas_call(
         functools.partial(whole_kernel, cfg),
         out_shape=(
-            jax.ShapeDtypeStruct((R, D), bf16),
-            jax.ShapeDtypeStruct((R, D), bf16),
+            jax.ShapeDtypeStruct((R, D), f32),
+            jax.ShapeDtypeStruct((R, D), f32),
         ),
-        in_specs=[vmem] * 13 + [hbm] * 8,
+        in_specs=[vmem] * 7 + [hbm] * 14,
         out_specs=(vmem, vmem),
         scratch_shapes=scratch,
         compiler_params=pltpu.CompilerParams(
@@ -1006,19 +1148,19 @@
         ),
         name="whole",
     )(
+        feature_forget_baseline.reshape(1, mix_width),
+        amend_speed_baseline.reshape(1, mix_width),
+        sudden_forget_extra.T,
+        group_scaling_factor.reshape(1, mix_width),
+        specialist_scaling_factor.reshape(1, D),
+        selected_specialists.T,
+        selection_mixing_factors.T,
+        specialist_tokens_activations,
         query_vectors,
         attend_lookup_vectors,
         attend_content_vectors,
         forget_speed_dependent,
         amend_speed_dependent,
-        feature_forget_baseline.reshape(1, mix_width),
-        amend_speed_baseline.reshape(1, mix_width),
-        sudden_forget_extra.T,
-        group_scaling_factor.reshape(1, mix_width),
-        specialist_tokens_activations,
-        specialist_scaling_factor.reshape(1, D),
-        selected_specialists.T,
-        selection_mixing_factors.T,
         result_switch_preactivation,
         result_mapping_matrix,
         dispatched_switch_matrix.reshape(D, ff),
@@ -1028,6 +1170,7 @@
         common_raising_matrix,
         common_lowering_matrix,
     )
+    return mix_sum.astype(bf16), moe_sum.astype(bf16)
 
 
 def solution(mesh):

time: 112 us -> 92.8 us (0.83)
  the two profiles are of different devices: /device:TPU:9 before, /device:TPU:0 now
where the time goes in v3:
time: 92.8 us; the launch traced here: 92.4 us
  Pallas kernels  88.7 us (96%)
  other arithmetic  3.03 us (3%)
    pallas_call x1, Pallas kernels, on_device(): pl.pallas_call(functools.partial(whole_kernel, cfg), out_shape=(jax.Shape...  88.7 us
    convert_element_type x2, other arithmetic, on_device(): return (mix_sum.astype(bf16), moe_sum.astype(bf16))  3.03 us

profile of v3, /device:TPU:0, one launch (start us, length us, event | category | flops | bytes accessed | tf_op | source)
XLA Modules:
  0.0 92.4 jit_solution(12407994364714419205)
XLA Ops:
  0.6 88.7 %whole.1 = (f32[128,2048]{1,0:T(8,128)}, f32[128,2048]{1,0:T(8,128)}) custom-call(f32[1,512]{1,0:T(1,128)} %bitcast.15, f32[1,512]{1,0:T(1,128)} %bitcast.16, f32[8,512]{1,0:T(8,128)} %bitcast.13, f32[1,512]{1,0:T(1,128)} %bitcast.17, f32[1,2048]{1,0:T(1,128)} %bitcast.14, s32[2,128]{1,0:T(2,128)} %bitcast.18, f32[2,128]{1,0:T(2,128)} %bitcast.19, ...), custom_call_target="tpu_custom_call" | custom-call | tf_op jit(solution)/shard_map/whole/pallas_call | solution.py:1137
  89.3 0.0 copy-start
  89.3 2.2 %convert_element_type.6 = bf16[128,2048]{1,0:T(8,128)(2,1)} convert(f32[128,2048]{1,0:T(8,128)} %get-tuple-element.4) | non-fusion elementwise | flops 262144 | bytes 1572864 | tf_op jit(solution)/shard_map/convert_element_type | solution.py:1173
  91.5 0.0 copy-done
  91.5 0.9 convert_element_type.7
Async XLA Ops:
  89.3 2.2 %copy-start = (f32[128,2048]{1,0:T(8,128)S(1)}, f32[128,2048]{1,0:T(8,128)}, u32[]{:S(2)}) copy-start(f32[128,2048]{1,0:T(8,128)} %get-tuple-element.5) | copy-start | bytes 3145732

commit v4 on v3

--- a/solution.py
+++ b/solution.py
@@ -377,17 +377,36 @@
 MESH = pl.DeviceIdType.MESH
 
 
+def pair_dot(left, right, dims=NN):
+    def one(x, y):
+        return lax.dot_general(x, y, dims, preferred_element_type=jnp.float32)
+
+    along = 0 if dims == NN else 1
+    wide = one(
+        jnp.concatenate([left[0], left[1]], axis=1),
+        jnp.concatenate([right[0], right[0]], axis=along),
+    )
+    return wide + one(left[0], right[1])
+
+
+def both_heads(parts, masks):
+    return tuple(
+        jnp.concatenate([part * mask for mask in masks], axis=0) for part in parts
+    )
+
+
 def span_step(heads, size, span, i, q_ref, k_ref, v_ref, f_ref, a_ref, fb_ref, ab_ref, extra_ref,
               flat_ref, memory_ref):
+    f32, bf16 = jnp.float32, jnp.bfloat16
+    pairs = range(heads // 2)
+    wide = 2 * size
     here = pl.ds(pl.multiple_of(i * span, span), span)
-    row = lax.broadcasted_iota(jnp.int32, (span, span), 0)
-    col = lax.broadcasted_iota(jnp.int32, (span, span), 1)
+    row = lax.broadcasted_iota(jnp.int32, (span, 2 * span), 0)
+    lane = lax.broadcasted_iota(jnp.int32, (span, 2 * span), 1)
+    col = jnp.where(lane >= span, lane - span, lane)
     eye = jnp.where(row == col, 1.0, 0.0)
-    below = jnp.where(row >= col, 1.0, 0.0)
-    row2 = lax.broadcasted_iota(jnp.int32, (2 * span, 2 * span), 0)
-    col2 = lax.broadcasted_iota(jnp.int32, (2 * span, 2 * span), 1)
-    col2 = jnp.where(col2 >= span, col2 - span, col2)
-    pair_mask = jnp.where(row2 >= span, row2 - span + 1, row2) > col2
+    below = row > col
+    upto = row >= col
     levels = []
     width = 1
     while width < span:
@@ -397,17 +416,30 @@
             & (col // width % 2 == 0)
         )
         width *= 2
-
-    q_all = q_ref[here, :].astype(jnp.float32)
-    k_all = k_ref[here, :].astype(jnp.float32)
-    v_all = v_ref[here, :].astype(jnp.float32)
-    rate_all = jax.nn.sigmoid(ab_ref[...] + a_ref[here, :].astype(jnp.float32))
-    speed = -jnp.exp(fb_ref[...] + f_ref[here, :].astype(jnp.float32))
+    side = lax.broadcasted_iota(jnp.int32, (span, wide), 1) < size
+    masks = (jnp.where(side, 1.0, 0.0).astype(bf16), jnp.where(side, 0.0, 1.0).astype(bf16))
+
+    def cut(array_in, p):
+        return array_in[:, p * wide : (p + 1) * wide]
+
+    q_all = q_ref[here, :].astype(f32)
+    k_all = k_ref[here, :].astype(f32)
+    rate_all = jax.nn.sigmoid(ab_ref[...] + a_ref[here, :].astype(f32))
+    speed = -jnp.exp(fb_ref[...] + f_ref[here, :].astype(f32))
     extra = extra_ref[here, :]
     decay_all = speed + jnp.concatenate(
-        [jnp.broadcast_to(extra[:, h : h + 1], (span, size)) for h in range(heads)], axis=1
-    )
-    cum_all = jnp.dot(below, decay_all, precision=highest, preferred_element_type=jnp.float32)
+        [jnp.where(side, extra[:, 2 * p : 2 * p + 1], extra[:, 2 * p + 1 : 2 * p + 2]) for p in pairs],
+        axis=1,
+    )
+    high, rest = split_two(decay_all)
+    rest = decay_all - high.astype(f32)
+    middle_part, low = split_two(rest)
+    tri = jnp.where(upto[:, :span], 1.0, 0.0).astype(bf16)
+    cum_all = jnp.dot(
+        jnp.concatenate([tri, tri, tri], axis=1),
+        jnp.concatenate([high, middle_part, low], axis=0),
+        preferred_element_type=f32,
+    )
     prev_all = cum_all - decay_all
     middle = cum_all[span // 2 : span // 2 + 1]
     last = cum_all[span - 1 : span]
@@ -420,57 +452,104 @@
     exp_last = jnp.exp(last)
     write_all = k_all * rate_all
     squares = k_all * k_all
-
-    every = range(heads)
-
-    def cut(array_in, h):
-        return array_in[:, h * size : (h + 1) * size]
-
-    norms = [lax.rsqrt(jnp.sum(cut(squares, h), -1, keepdims=True) + 1e-06) for h in every]
-    unit_all = k_all * jnp.concatenate(
-        [jnp.broadcast_to(n, (span, size)) for n in norms], axis=1
-    )
+    norms = []
+    for p in pairs:
+        square = cut(squares, p)
+        first = jnp.sum(jnp.where(side, square, 0.0), -1, keepdims=True)
+        second = jnp.sum(jnp.where(side, 0.0, square), -1, keepdims=True)
+        norms.append(lax.rsqrt(jnp.where(side, first, second) + 1e-06))
+    unit_all = k_all * jnp.concatenate(norms, axis=1)
     erase_all = unit_all * rate_all
-    left_all = jnp.concatenate([-unit_all * exp_prev_mid, q_all * exp_cum_mid], axis=0)
-    right_all = jnp.concatenate([erase_all * exp_mid_cum, write_all * exp_mid_cum], axis=0)
-    read_all = jnp.concatenate([-unit_all * exp_prev, q_all * exp_cum], axis=0)
-    tail_all = jnp.concatenate([erase_all * exp_tail, write_all * exp_tail], axis=0)
-    left_all, right_all = split_two(left_all), split_two(right_all)
-    read_all, tail_all = split_two(read_all), split_two(tail_all)
-
-    def cut2(parts, h):
-        return tuple(cut(part, h) for part in parts)
-
-    pairs = [
-        jnp.where(pair_mask, dot_parts(cut2(left_all, h), cut2(right_all, h), NT), 0.0)
-        for h in every
-    ]
-    strict = [p[:span, :span] for p in pairs]
+    left_all = split_two(jnp.concatenate([-unit_all * exp_prev_mid, q_all * exp_cum_mid], axis=0))
+    read_all = split_two(jnp.concatenate([-unit_all * exp_prev, q_all * exp_cum], axis=0))
+    erase_mid, write_mid = split_two(erase_all * exp_mid_cum), split_two(write_all * exp_mid_cum)
+    tail_all = split_two(jnp.concatenate([erase_all * exp_tail, write_all * exp_tail], axis=0))
+
+    def cuts(parts, p):
+        return tuple(cut(part, p) for part in parts)
+
+    scores = []
+    for p in pairs:
+        right = tuple(
+            jnp.concatenate([x, y], axis=0)
+            for x, y in zip(
+                both_heads(cuts(erase_mid, p), masks), both_heads(cuts(write_mid, p), masks)
+            )
+        )
+        scores.append(pair_dot(cuts(left_all, p), right, NT))
+    strict = [jnp.where(below, s[:span, :wide], 0.0) for s in scores]
+    by_write = [split_two(jnp.where(below, s[:span, wide:], 0.0)) for s in scores]
+    ask_erase = [split_two(jnp.where(upto, s[span:, :wide], 0.0)) for s in scores]
+    ask_write = [split_two(jnp.where(upto, s[span:, wide:], 0.0)) for s in scores]
     solved = [eye + jnp.where(levels[0], s, 0.0) for s in strict]
     for level in levels[1:]:
         halves = [split_two(x) for x in solved]
         middles = [
-            dot_parts(split_two(jnp.where(level, s, 0.0)), x, NN) for s, x in zip(strict, halves)
+            pair_dot(split_two(jnp.where(level, s, 0.0)), both_heads(x, masks))
+            for s, x in zip(strict, halves)
         ]
         solved = [
-            x + dot_parts(xs, split_two(m), NN) for x, xs, m in zip(solved, halves, middles)
+            x + pair_dot(xs, both_heads(split_two(m), masks))
+            for x, xs, m in zip(solved, halves, middles)
         ]
-    memories = [memory_ref[h] for h in every]
-    reads = [dot_parts(cut2(read_all, h), split_two(memories[h]), NT) for h in every]
-    blank = jnp.zeros((span, size), jnp.float32)
-    values = [jnp.concatenate([cut(v_all, h), blank], axis=1) for h in every]
-    rights = [
-        reads[h][:span] + dot3(pairs[h][:span, span:], values[h]) for h in every
-    ]
-    updates = [dot3(solved[h], rights[h]) for h in every]
-    stacked = [jnp.concatenate([updates[h], values[h]], axis=0) for h in every]
-    for h in every:
-        flat_ref[here, 2 * size * h : 2 * size * (h + 1)] = reads[h][span:] + dot3(
-            pairs[h][span:], stacked[h]
-        )
-    for h in every:
-        memory_ref[h] = memories[h] * cut(exp_last, h) + dot_parts(
-            split_two(stacked[h].T), cut2(tail_all, h), NN
+    memories = [memory_ref[p] for p in pairs]
+    reads = []
+    for p in pairs:
+        kept = split_two(memories[p])
+        right = tuple(
+            jnp.concatenate(
+                [part[:size] * masks[0], part[:size] * masks[1],
+                 part[size:] * masks[0], part[size:] * masks[1]], axis=0
+            )
+            for part in kept
+        )
+        reads.append(pair_dot(cuts(read_all, p), right, NT))
+    values = [cut(v_ref[here, :], p) for p in pairs]
+    stacked_values = [both_heads((v,), masks)[0] for v in values]
+
+    def times_values(parts, p):
+        return jnp.dot(
+            jnp.concatenate(parts, axis=1),
+            jnp.concatenate([stacked_values[p], stacked_values[p]], axis=0),
+            preferred_element_type=f32,
+        )
+
+    updates = []
+    for p in pairs:
+        first = split_two(reads[p][:span, :wide] + times_values(by_write[p], p))
+        second = split_two(reads[p][:span, wide:])
+        right = tuple(
+            jnp.concatenate([x, y], axis=1)
+            for x, y in zip(both_heads(first, masks), both_heads(second, masks))
+        )
+        updates.append(pair_dot(split_two(solved[p]), right))
+    for p in pairs:
+        halves = split_two(updates[p])
+        right = tuple(
+            jnp.concatenate([x, y], axis=1)
+            for x, y in zip(
+                both_heads(tuple(h[:, :wide] for h in halves), masks),
+                both_heads(tuple(h[:, wide:] for h in halves), masks),
+            )
+        )
+        total = reads[p][span:] + pair_dot(ask_erase[p], right)
+        flat_ref[here, 2 * wide * p : 2 * wide * p + wide] = total[:, :wide] + times_values(
+            ask_write[p], p
+        )
+        flat_ref[here, 2 * wide * p + wide : 2 * wide * (p + 1)] = total[:, wide:]
+    for p in pairs:
+        tail = cuts(tail_all, p)
+        stacked = jnp.concatenate([updates[p][:, :wide], values[p].astype(f32)], axis=0)
+        grown = pair_dot(split_two(stacked.T), tail)
+        turned = pair_dot(
+            split_two(updates[p][:, wide:].T), tuple(part[:span] for part in tail)
+        )
+        fade = cut(exp_last, p)
+        memory_ref[p, :size] = memories[p][:size] * fade + jnp.where(
+            side[:size], grown[:size], grown[size:]
+        )
+        memory_ref[p, size:] = memories[p][size:] * fade + jnp.where(
+            side[:size], turned[:size], turned[size:]
         )
 
 
@@ -480,7 +559,7 @@
     tok_hbm, q_hbm, k_hbm, v_hbm, f_hbm, a_hbm,
     gate_hbm, map_hbm, gw_hbm, uw_hbm, dw_hbm, cg_hbm, cu_hbm, cd_hbm,
     mix_out, moe_out,
-    xg, wg, flat, memory, parts, state, mixed, mp, mc, mx,
+    xg, wg, flat, memory, parts, mixed, mp, mc, mx,
     part, rc, zb, extra_v, hid, hall, hpack,
     tok_ref, q_ref, k_ref, v_ref, f_ref, a_ref,
     gate_v, map_v, gw_v, uw_v, dw_v, cg_v, cu_v, cd_v,
@@ -594,10 +673,10 @@
 
         return view
 
-    def by_cols(n, flip):
+    def by_cols(n):
         def view(ref, gg):
             cols = ref.shape[1] // 4
-            unit = 2 * n + (1 - gg if flip else gg)
+            unit = 2 * n + gg
             return ref.at[:, pl.ds(pl.multiple_of(unit * cols, cols), cols)]
 
         return view
@@ -605,12 +684,10 @@
     pieces = [
         (gw_hbm, gw_v, by_rows(2, 0)), (gw_hbm, gw_v, by_rows(2, 1)),
         (uw_hbm, uw_v, by_rows(2, 0)), (uw_hbm, uw_v, by_rows(2, 1)),
-        (dw_hbm, dw_v, by_cols(0, False)), (dw_hbm, dw_v, by_cols(1, False)),
-        (dw_hbm, dw_v, by_cols(1, True)),
+        (dw_hbm, dw_v, by_cols(0)), (dw_hbm, dw_v, by_cols(1)),
         (cg_hbm, cg_v, by_rows(1, 0)), (cu_hbm, cu_v, by_rows(1, 0)),
         (cd_hbm, cd_v, by_rows(1, 0)),
     ]
-    handed = (0, 1, 2, 3, 4, 7, 8, 9)
 
     def wx(p):
         src, dst, view = pieces[p]
@@ -662,11 +739,14 @@
     for copy in locals_[1:6]:
         copy.wait()
 
-    mrow = lax.broadcasted_iota(jnp.int32, (2 * size, size), 0)
-    mcol = lax.broadcasted_iota(jnp.int32, (2 * size, size), 1)
-    begin = jnp.where(mrow == mcol + size, 1.0, 0.0)
-    for h in range(heads):
-        memory[h] = begin
+    wide = 2 * size
+    mrow = lax.broadcasted_iota(jnp.int32, (wide, wide), 0)
+    mcol = lax.broadcasted_iota(jnp.int32, (wide, wide), 1)
+    begin = jnp.where(mrow == jnp.where(mcol < size, mcol + size, mcol), 1.0, 0.0)
+    for p in range(heads // 2):
+        memory[p] = begin * jnp.where(mrow >= size, 1.0, 0.0)
+    side = lax.broadcasted_iota(jnp.int32, (size, wide), 1) < size
+    masks = (jnp.where(side, 1.0, 0.0).astype(bf16), jnp.where(side, 0.0, 1.0).astype(bf16))
 
     def during(part_of):
         return min(steps - 1, (part_of * steps) // 8)
@@ -674,7 +754,7 @@
     hops = [(during(3), gather_z, 0), (during(6), gather_z, 1)]
     hops = [hop for hop in hops if hop[2] < last]
     hops += [(during(2), pass_on, 0), (during(4), pass_on, 1), (during(5), pass_on, 2),
-             (during(6), pass_on, 3)]
+             (during(6), pass_on, 3), (during(7), pass_on, 4)]
     early = len([hop for hop in hops if hop[1] is gather_z])
 
     @pl.loop(0, steps)
@@ -696,54 +776,56 @@
     def st_step(first):
         if not first:
             st_copy().wait_recv()
-        for h in range(heads):
-            after = memory[h, :size]
+        for p in range(heads // 2):
+            after = memory[p, :size]
             if not first:
-                before = parts[1, h]
-                carry = split_two(memory[h, size:])
+                carry = both_heads(split_two(memory[p, size:]), masks)
                 after = after + (
-                    jnp.dot(before, carry[0], preferred_element_type=f32)
-                    + jnp.dot(before, carry[1], preferred_element_type=f32)
+                    jnp.dot(parts[1, p], carry[0], preferred_element_type=f32)
+                    + jnp.dot(parts[1, p], carry[1], preferred_element_type=f32)
                 )
-            parts[0, h] = after.astype(bf16)
+            parts[0, p] = after.astype(bf16)
         pl.when(e < last)(lambda: st_copy().start())
 
     pl.when(e == 0)(lambda: st_step(True))
-    pass_on(4)
-    for k in range(early, last):
-        gather_z(k)
     pl.when(e == 1)(lambda: st_step(False))
 
     def finish_step(i):
         here = pl.ds(pl.multiple_of(i * span, span), span)
         centered_all = []
-        for h in range(heads):
-            pane = flat[here, 2 * size * h : 2 * size * (h + 1)]
-            head_out = pane[:, :size]
-            left = split_two(pane[:, size:])
-            head_out = head_out + (
-                lax.dot_general(left[0], state[h], NT, preferred_element_type=f32)
-                + lax.dot_general(left[1], state[h], NT, preferred_element_type=f32)
+        here_side = lax.broadcasted_iota(jnp.int32, (span, wide), 1) < size
+
+        def mean_of(values):
+            first = jnp.sum(jnp.where(here_side, values, 0.0), -1, keepdims=True)
+            second = jnp.sum(jnp.where(here_side, 0.0, values), -1, keepdims=True)
+            return jnp.where(here_side, first, second) / size
+
+        for p in range(heads // 2):
+            left = split_two(flat[here, 2 * wide * p + wide : 2 * wide * (p + 1)])
+            stack = both_heads((parts[1, p],), masks)[0]
+            pair_out = flat[here, 2 * wide * p : 2 * wide * p + wide] + lax.dot_general(
+                jnp.concatenate(left, axis=1), jnp.concatenate([stack, stack], axis=1), NT,
+                preferred_element_type=f32,
             )
-            centered = head_out - jnp.mean(head_out, -1, keepdims=True)
-            head_var = jnp.mean(centered * centered, -1, keepdims=True)
-            centered_all.append(centered * lax.rsqrt(head_var + 0.00064))
+            centered = pair_out - mean_of(pair_out)
+            centered_all.append(centered * lax.rsqrt(mean_of(centered * centered) + 0.00064))
         scaled = jnp.concatenate(centered_all, axis=1) * gain_ref[...]
         gate = jax.nn.sigmoid(gate_v[here, :].astype(f32))
         mixed[here, :] = (scaled * gate).astype(bf16)
 
-    def finish():
-        locals_[6].wait()
-
-        @pl.when(e == 0)
-        def _():
-            state[...] = jnp.zeros_like(state)
-
-        @pl.when(e > 0)
-        def _():
-            state[...] = parts[1]
-
-        pl.loop(0, steps)(finish_step)
+    def finish(low, high):
+        pl.loop(low, high)(finish_step)
+
+    locals_[6].wait()
+
+    @pl.when(e == 0)
+    def _():
+        for p in range(heads // 2):
+            parts[1, p] = jnp.zeros((size, wide), bf16)
+
+    ahead = jnp.where(e <= 1, steps // 2, 0)
+    finish(0, ahead)
+    pass_on(5)
 
 
     def md_copy(xx):
@@ -783,14 +865,13 @@
         add_rows(away, [away, block(mc, 1 - x)])
         mx_copy().start()
 
-    for copy in locals_[8:]:
-        copy.wait()
-    for ee in range(E):
-        ds_wait(ee)
-    for n in range(len(column)):
-        w_wait(n)
-    for p in range(4):
-        wy_wait(p)
+    def ready():
+        for copy in locals_[8:]:
+            copy.wait()
+        for n in range(len(column)):
+            w_wait(n)
+        for p in range(4):
+            wy_wait(p)
 
     W = D // 2
 
@@ -882,9 +963,13 @@
                 )
 
     def dest_of(k):
-        low = jnp.where(k < last - e, last - k, k - (last - e))
-        high = jnp.where(k < e, k, last - (k - e))
-        return jnp.where(k == last, e, jnp.where(e < E // 2, low, high))
+        low = e < E // 2
+        near = jnp.where(low, e, last - e)
+        right = last - 1 - near
+        rest = jnp.where(k - 2 < right, last + 1 - k, k - 1 - right)
+        inner = jnp.where(k == 0, last, jnp.where(k == 1, 0, rest))
+        pick = jnp.where(k == last, near, jnp.where(near == 0, last - k, inner))
+        return jnp.where(low, pick, last - pick)
 
     edge = (e == 0) | (e == last)
 
@@ -927,68 +1012,65 @@
         )
         z_copy(dest, half).start()
 
-    def experts(half):
+    def middle(k, half):
+        pl.when(jnp.logical_not(edge))(lambda: middle_step(dest_of(k), half))
+
+    def hidden(k):
+        dest = dest_of(k)
+        ds_wait(dest)
+        hidden_rows(dest)
+        if k < last:
+            pl.when(edge)(lambda: pack_rows(dest))
+
+    ready()
+    for k in range(last - 1, 0, -1):
+        hidden(k)
+    pl.when(e == 2)(lambda: st_step(False))
+    for k in range(early, last):
+        gather_z(k)
+    hidden(0)
+    wy_wait(4)
+
+    def share(n):
+        k, half = n // 2, n % 2
+
         @pl.when(edge)
         def _():
-            @pl.loop(0, last)
-            def _(k):
-                dest = dest_of(k)
-                if half == 0:
-                    hidden_rows(dest)
-                    pack_rows(dest)
-
-                    @pl.when(k > 0)
-                    def _():
-                        edge_step(dest_of(k - 1), half)
-
-                part_rows(dest, half, rows=cap)
-                rd_copy(dest, half, cap).start()
-                if half:
-                    @pl.when(k > 0)
-                    def _():
-                        edge_step(dest_of(k - 1), half)
-
-            if half == 0:
-                hidden_rows(e)
-            edge_step(dest_of(last - 1), half)
+            part_rows(dest_of(k), half, rows=cap)
+            rd_copy(dest_of(k), half, cap).start()
 
         @pl.when(jnp.logical_not(edge))
         def _():
-            @pl.loop(0, last)
-            def _(k):
-                dest = dest_of(k)
-                if half == 0:
-                    hidden_rows(dest)
-                part_rows(dest, half)
-                rd_copy(dest, half).start()
-
-            if half == 0:
-                hidden_rows(e)
-
-    def middle(k, half):
-        pl.when(jnp.logical_not(edge))(lambda: middle_step(dest_of(k), half))
-
-    wy_wait(4)
-    experts(0)
-    pl.when(e == 2)(lambda: st_step(False))
-    wx(5).wait_recv()
-    wx(6).wait_recv()
-    experts(1)
+            part_rows(dest_of(k), half)
+            rd_copy(dest_of(k), half).start()
+
+    def send_on(n):
+        pl.when(edge)(lambda: edge_step(dest_of(n // 2), n % 2))
+
+    share(0)
+    pass_on(6)
+    send_on(0)
+    wy_wait(5)
+    for n in range(1, 2 * last):
+        share(n)
+        if n > 1:
+            send_on(n - 1)
+    hidden(last)
+    send_on(2 * last - 1)
     pl.when(e > 2)(lambda: st_step(False))
+    pass_on(7)
     middle(0, 0)
-    finish()
-    pass_on(7)
-    for k in range(1, last):
-        middle(k, 0)
-    mixer_out()
+    finish(ahead, steps)
     pass_on(8)
     middle(0, 1)
-    pass_on(9)
-    for k in range(1, last):
-        middle(k, 1)
-    for p in (7, 8, 9):
-        wy_wait(p)
+    mixer_out()
+    for half in range(2):
+        for k in range(1, last):
+            middle(k, half)
+    wy_wait(6)
+    wy_wait(7)
     hidden_rows(e, True)
+    wy_wait(8)
     for half in range(2):
         part_rows(e, half, True)
         rd_copy(e, half).start()
@@ -1013,7 +1095,6 @@
         w_copy(n).wait_send()
     for p in range(len(pieces)):
         wx(p).wait_send()
-    for p in handed:
         wy(p).wait_send()
     pl.when(e < last)(lambda: st_copy().wait_send())
     for xx in range(X):
@@ -1063,7 +1144,7 @@
     ff = dispatched_switch_matrix.shape[2]
     sff = common_switch_matrix.shape[1]
     gathered = E * T * R * D * 2
-    if T != 4 or lax.axis_size("grp") != 2 or gathered > 12_000_000 or tokens != T * R or E < 2:
+    if heads % 2 or span != size or T != 4 or lax.axis_size("grp") != 2 or gathered > 12_000_000 or tokens != T * R or E < 2 or 2 * size != 128:
         return collective_plan(
             query_vectors,
             attend_lookup_vectors,
@@ -1099,9 +1180,8 @@
         pltpu.VMEM((E * 2 * R, D), bf16),
         pltpu.VMEM((E * 2, wrows, R), f32),
         pltpu.VMEM((tokens, 2 * mix_width), f32),
-        pltpu.VMEM((heads, 2 * size, size), f32),
-        pltpu.VMEM((2, heads, size, size), bf16),
-        pltpu.VMEM((heads, size, size), bf16),
+        pltpu.VMEM((heads // 2, 2 * size, 2 * size), f32),
+        pltpu.VMEM((2, heads // 2, size, 2 * size), bf16),
         pltpu.VMEM((tokens, mix_width), bf16),
         pltpu.VMEM((T * R, D), bf16),
         pltpu.VMEM((2 * R, D), bf16),
@@ -1130,7 +1210,7 @@
         dma((14,)),
         dma((2, E)), dma((2, E)), dma((E,)), dma((E,)), dma((2 * E,)), dma((2 * E,)),
         dma((1,)), dma((1,)),
-        dma((10,)), dma((10,)), dma((10,)), dma((10,)),
+        dma((9,)), dma((9,)), dma((9,)), dma((9,)),
         dma((2,)), dma((2,)), dma((1,)), dma((1,)),
         dma((E, 2)), dma((E, 2)), dma((2 * E, 2)), dma((2 * E, 2)),
     ]

time: 92.8 us -> 86.8 us (0.935)
  Pallas kernels: 88.7 us -> 82.9 us
    pallas_call x1, Pallas kernels: 88.7 us -> 82.9 us  [on_device(): pl.pallas_call(functools.partial(whole_kernel, cfg), out_shape=(jax.Shape...]
where the time goes in v4:
time: 86.8 us; the launch traced here: 86.6 us
  Pallas kernels  82.9 us (96%)
  other arithmetic  3.03 us (3%)
    pallas_call x1, Pallas kernels, on_device(): pl.pallas_call(functools.partial(whole_kernel, cfg), out_shape=(jax.Shape...  82.9 us
    convert_element_type x2, other arithmetic, on_device(): return (mix_sum.astype(bf16), moe_sum.astype(bf16))  3.03 us

profile of v4, /device:TPU:0, one launch (start us, length us, event | category | flops | bytes accessed | tf_op | source)
XLA Modules:
  0.0 86.6 jit_solution(4948949364611443239)
XLA Ops:
  0.6 82.9 %whole.1 = (f32[128,2048]{1,0:T(8,128)}, f32[128,2048]{1,0:T(8,128)}) custom-call(f32[1,512]{1,0:T(1,128)} %bitcast.15, f32[1,512]{1,0:T(1,128)} %bitcast.16, f32[8,512]{1,0:T(8,128)} %bitcast.13, f32[1,512]{1,0:T(1,128)} %bitcast.17, f32[1,2048]{1,0:T(1,128)} %bitcast.14, s32[2,128]{1,0:T(2,128)} %bitcast.18, f32[2,128]{1,0:T(2,128)} %bitcast.19, ...), custom_call_target="tpu_custom_call" | custom-call | tf_op jit(solution)/shard_map/whole/pallas_call | solution.py:1217
  83.6 0.0 copy-start
  83.6 2.2 %convert_element_type.6 = bf16[128,2048]{1,0:T(8,128)(2,1)} convert(f32[128,2048]{1,0:T(8,128)} %get-tuple-element.4) | non-fusion elementwise | flops 262144 | bytes 1572864 | tf_op jit(solution)/shard_map/convert_element_type | solution.py:1253
  85.8 0.0 copy-done
  85.8 0.9 convert_element_type.7
Async XLA Ops:
  83.6 2.2 %copy-start = (f32[128,2048]{1,0:T(8,128)S(1)}, f32[128,2048]{1,0:T(8,128)}, u32[]{:S(2)}) copy-start(f32[128,2048]{1,0:T(8,128)} %get-tuple-element.5) | copy-start | bytes 3145732
